TPU v7x, 32 devices: a whole 2x2x4 slice. The times are simulated.
32 devices in a mesh: grp: 2 (over y), sp: 4 (over z), fs: 2 (over x), tp: 2 (over core).
Axes of the slice: x: 2, y: 2, z: 4, core: 2. Of those that a mesh axis runs over, the one named last changes fastest.
Arguments:
- tokens: bfloat16 [4, 512, 2048], P(('grp', 'fs'), 'sp'), parts along dimension 0, may hold values from -6 to 6
- norm_gain: float32 [2048], replicated, may hold values from 0.1 to 1.9
- query_attend: bfloat16 [2048, 8, 128], P(None, ('fs', 'tp')), may hold values from -0.125 to 0.125
- key_attend: bfloat16 [2048, 8, 128], P(None, ('fs', 'tp')), may hold values from -0.125 to 0.125
- value_attend: bfloat16 [2048, 8, 128], P(None, ('fs', 'tp')), may hold values from -0.125 to 0.125
- query_linear: bfloat16 [2048, 8, 128], P(None, ('fs', 'tp')), may hold values from -0.125 to 0.125
- key_linear: bfloat16 [2048, 8, 128], P(None, ('fs', 'tp')), may hold values from -0.125 to 0.125
- value_linear: bfloat16 [2048, 8, 256], P(None, ('fs', 'tp')), may hold values from -0.125 to 0.125
- decay_down: bfloat16 [2048, 32], replicated, may hold values from -0.125 to 0.125
- decay_up: bfloat16 [32, 8, 128], replicated, may hold values from -2.109375 to 2.109375
- decay_bias: float32 [8, 128], replicated, may hold values from -1.5 to 7.5
- log_retain: float32 [4, 512, 8], P(('grp', 'fs'), 'sp'), parts along dimension 0, may hold values from -1.5 to 0
- query_gain: float32 [64], replicated, may hold values from 0.6 to 4
- key_gain: float32 [8, 2, 64], replicated, may hold values from 0.8 to 14
- diff_lambda: float32 [8], replicated, may hold values from 0.3 to 0.8
- mix_gain: float32 [128], replicated, may hold values from 0.1 to 1.9
- state_gain: float32 [256], replicated, may hold values from 0.1 to 1.9
- init_state: float32 [4, 8, 128, 256], P('grp', ('fs', 'tp')), parts along dimension 0, may hold values from -80 to 80
- output_attend: bfloat16 [1024, 2048], P(None, 'tp'), may hold values from -0.109375 to 0.109375
- output_linear: bfloat16 [2048, 2048], P(None, 'tp'), may hold values from -0.109375 to 0.109375
Outputs:
- mixed_out: bfloat16 [4, 512, 2048], P(('grp', 'fs'), 'sp', 'tp'), parts along dimension 0
There are 2 independent parts, one for each index of `grp`. A program takes and returns all parts, laid end to end along the dimension named above; an argument that names none is the same for every part. Nothing has to cross between parts.
All inputs are finite; a program needn't handle non-finite values.
Results may differ from a plain program's by a relative error of at most 0.018.
The roundings to bfloat16 on the way count: a program that leaves them out, or rounds other values in their place, can miss the bound.
Values may be sent and summed in bfloat16 or wider, within the bound.
A program may use at most 128 MiB of HBM per device.

v0:
```python
import jax
import jax.numpy as jnp
from jax import lax
from jax.sharding import PartitionSpec as P

MIXER_HEADS = 8
HD_A = 64
DV_A = 128
HDK = 128
HDV = 256
BLK = 64


norm_eps = 1e-06
decay_tau = 16.0


def entering(part, axis, combine, identity):
    place = lax.axis_index(axis)
    gathered = jax.tree.map(lambda a: lax.all_gather(a, axis), part)
    state = jax.tree.map(lambda a, e: jnp.zeros_like(a) + jnp.asarray(e, a.dtype), part, identity)

    def one(hop, state):
        return combine(
            state, jax.tree.map(lambda a: lax.dynamic_index_in_dim(a, hop, 0, False), gathered)
        )

    return lax.fori_loop(0, place, one, state)


def rms_scale(values, gain):
    widened = values.astype(jnp.float32)
    return (
        widened * lax.rsqrt(jnp.mean(widened * widened, axis=-1, keepdims=True) + norm_eps) * gain
    )


def head_order(fs_size, tp_size, tp_rank):
    per_device = MIXER_HEADS // (fs_size * tp_size)
    owners = jnp.arange(fs_size, dtype=jnp.int32)[:, None] * tp_size + tp_rank
    return (owners * per_device + jnp.arange(per_device, dtype=jnp.int32)[None, :]).reshape(-1)


def linear_blocks(queries, keys_in, values_in, log_decay):
    tok_rows, head_count, key_dim = queries.shape
    value_dim = values_in.shape[-1]
    block_count = tok_rows // BLK
    highest_precision = lax.Precision.HIGHEST

    def split_blocks(source):
        return source.reshape(block_count, BLK, head_count, source.shape[-1])

    causal = (
        jnp.arange(BLK, dtype=jnp.int32)[:, None] >= jnp.arange(BLK, dtype=jnp.int32)[None, :]
    )[None]

    def advance(carry, inputs_now):
        recurrent_state, offset = carry
        question_patch_lines, block_k, value_tile_width, block_log = inputs_now
        running_state = jnp.cumsum(block_log, axis=0)
        pivot = running_state[BLK // 2]
        q_scaled = question_patch_lines * jnp.exp(running_state - pivot[None])
        k_scaled = block_k * jnp.exp(pivot[None] - running_state)
        scores = jnp.einsum("thk,shk->hts", q_scaled, k_scaled, precision=highest_precision)
        scores = jnp.where(causal, scores, 0.0)
        inside_block = jnp.einsum(
            "hts,shv->thv", scores, value_tile_width, precision=highest_precision
        )
        inside_block = inside_block + jnp.einsum(
            "jwo,wos->jws",
            question_patch_lines * jnp.exp(running_state),
            recurrent_state,
            precision=highest_precision,
        )
        final_state = running_state[-1]
        faded_memory_matrix = block_k * jnp.exp(final_state[None] - running_state)
        recurrent_state = recurrent_state * jnp.exp(final_state)[:, :, None] + jnp.einsum(
            "zcb,zcw->cbw", faded_memory_matrix, value_tile_width, precision=highest_precision
        )
        reaching_keys = question_patch_lines * jnp.exp(offset[None] + running_state)
        return ((recurrent_state, offset + final_state), (inside_block, reaching_keys))

    start_carry = (
        jnp.zeros((head_count, key_dim, value_dim), jnp.float32),
        jnp.zeros((head_count, key_dim), jnp.float32),
    )
    (recurrent_state, total_decay), (inside_block, reaching_keys) = lax.scan(
        advance,
        start_carry,
        (
            split_blocks(queries),
            split_blocks(keys_in),
            split_blocks(values_in),
            split_blocks(log_decay),
        ),
    )
    return (
        recurrent_state,
        total_decay,
        inside_block.reshape(tok_rows, head_count, value_dim),
        reaching_keys.reshape(tok_rows, head_count, key_dim),
    )


def body(
    tokens,
    norm_gain,
    query_attend,
    key_attend,
    value_attend,
    query_linear,
    key_linear,
    value_linear,
    decay_down,
    decay_up,
    decay_bias,
    log_retain,
    query_gain,
    key_gain,
    diff_lambda,
    mix_gain,
    state_gain,
    init_state,
    output_attend,
    output_linear,
):
    fs_size = lax.axis_size("fs")
    tp_size = lax.axis_size("tp")
    tp_rank = lax.axis_index("tp")
    tok_rows = tokens.shape[1]
    normed = rms_scale(tokens, norm_gain).astype(jnp.bfloat16)
    normed_rows = normed[0]
    local_weights = (query_attend, key_attend, value_attend, query_linear, key_linear, value_linear)
    widths = [weight.shape[1] * weight.shape[2] for weight in local_weights]
    packed = jnp.concatenate(
        [weight.reshape(weight.shape[0], -1) for weight in local_weights], axis=1
    )
    computed = jnp.einsum(
        "std,dp->stp",
        lax.all_gather(normed, "fs", axis=0, tiled=True),
        packed,
        preferred_element_type=jnp.float32,
    ).astype(jnp.bfloat16)
    arrived = lax.all_to_all(computed, "fs", split_axis=0, concat_axis=2, tiled=True).reshape(
        tok_rows, fs_size, -1
    )
    sections = []
    column_at = 0
    for weight, width_now in zip(local_weights, widths):
        section = arrived[:, :, column_at : column_at + width_now]
        sections.append(section.reshape(tok_rows, fs_size * weight.shape[1], weight.shape[2]))
        column_at = column_at + width_now
    projected = tuple(sections)
    q_pair, k_pair, v_attend, q_lin, k_lin, v_lin = projected
    head_ids = head_order(fs_size, tp_size, tp_rank)
    head_count = head_ids.shape[0]
    q_unit = rms_scale(q_pair.reshape(tok_rows, head_count, 2, HD_A), query_gain).astype(
        jnp.bfloat16
    )
    k_unit = rms_scale(
        k_pair.reshape(tok_rows, head_count, 2, HD_A), jnp.take(key_gain, head_ids, axis=0)
    ).astype(jnp.bfloat16)
    sp_start = lax.axis_index("sp") * tok_rows
    query_block = (sp_start + jnp.arange(tok_rows, dtype=jnp.int32)) // BLK
    score_scale = HD_A ** (-0.5)
    blank_attend = (
        jnp.full((head_count, 2, tok_rows), -jnp.inf, jnp.float32),
        jnp.zeros((head_count, 2, tok_rows), jnp.float32),
        jnp.zeros((head_count, 2, tok_rows, DV_A), jnp.float32),
    )
    carry = blank_attend
    seg_keys = lax.all_gather(k_unit, "sp", axis=0, tiled=True)
    seg_values = lax.all_gather(v_attend, "sp", axis=0, tiled=True)
    span = seg_keys.shape[0]
    stride_token_lines = 2 * tok_rows
    step_count = span // stride_token_lines
    key_steps = seg_keys.reshape(step_count, stride_token_lines, head_count, 2, HD_A)
    value_steps = seg_values.reshape(step_count, stride_token_lines, head_count, DV_A)

    def one_step(running_state, inputs_now):
        step_index, key_step, value_step = inputs_now
        key_start = step_index * stride_token_lines

        def compute(current):
            run_max, run_total, run_acc = current
            scores = (
                jnp.einsum("qhmd,khmd->hmqk", q_unit, key_step, preferred_element_type=jnp.float32)
                * score_scale
            )
            key_block = (key_start + jnp.arange(stride_token_lines, dtype=jnp.int32)) // BLK
            allowed = query_block[:, None] >= key_block[None, :]
            scores = jnp.where(allowed, scores, -jnp.inf)
            new_max = jnp.maximum(run_max, jnp.max(scores, axis=-1))
            factor = jnp.exp(run_max - new_max)
            raised = jnp.exp(scores - new_max[..., None])
            run_total = run_total * factor + jnp.sum(raised, axis=-1)
            run_acc = run_acc * factor[..., None] + jnp.einsum(
                "hmqk,khv->hmqv",
                raised.astype(jnp.bfloat16),
                value_step,
                preferred_element_type=jnp.float32,
            )
            return (new_max, run_total, run_acc)

        def unchanged(current):
            return current

        return (lax.cond(key_start <= sp_start, compute, unchanged, running_state), None)

    carry, _ = lax.scan(
        one_step, carry, (jnp.arange(step_count, dtype=jnp.int32), key_steps, value_steps)
    )
    run_max, run_total, run_acc = carry
    lambda_heads = jnp.take(diff_lambda, head_ids, axis=0)
    diff_raw = (
        run_acc[:, 0] / run_total[:, 0, :, None]
        - lambda_heads[:, None, None] * run_acc[:, 1] / run_total[:, 1, :, None]
    )
    attend_out = rms_scale(jnp.transpose(diff_raw, (1, 0, 2)), mix_gain).astype(jnp.bfloat16)
    low_rank = jnp.dot(normed_rows, decay_down, preferred_element_type=jnp.float32).astype(
        jnp.bfloat16
    )
    up_columns = jnp.take(decay_up, head_ids, axis=1)
    pre_act = jnp.einsum(
        "tr,rhk->thk", low_rank, up_columns, preferred_element_type=jnp.float32
    ) + jnp.take(decay_bias, head_ids, axis=0)
    retain_heads = jnp.take(log_retain[0], head_ids, axis=1)
    log_decay = jax.nn.log_sigmoid(pre_act) / decay_tau + retain_heads[:, :, None]
    local_state, local_decay, inside_block, reaching_keys = linear_blocks(
        q_lin.astype(jnp.float32) * HDK ** (-0.5),
        k_lin.astype(jnp.float32),
        v_lin.astype(jnp.float32),
        log_decay,
    )

    def chain(earlier, later):
        return (earlier[0] + later[0], earlier[1] * jnp.exp(later[0])[:, :, None] + later[1])

    zero_chain = (jnp.zeros_like(local_decay), jnp.zeros_like(local_state))
    prior_decay, prior_state = entering((local_decay, local_state), "sp", chain, zero_chain)
    start_state = lax.all_to_all(init_state, "fs", split_axis=0, concat_axis=1, tiled=True)[0]
    incoming_state = start_state * jnp.exp(prior_decay)[:, :, None] + prior_state
    linear_raw = inside_block + jnp.einsum(
        "jwo,wos->jws", reaching_keys, incoming_state, precision=lax.Precision.HIGHEST
    )
    linear_out = rms_scale(linear_raw, state_gain).astype(jnp.bfloat16)
    out_cols = output_attend.shape[1]
    per_device = MIXER_HEADS // (fs_size * tp_size)
    attend_view = output_attend.reshape(fs_size, tp_size, per_device * DV_A, out_cols)
    linear_view = output_linear.reshape(fs_size, tp_size, per_device * HDV, out_cols)
    blank_out = jnp.zeros((tok_rows, out_cols), jnp.float32)
    running_out = blank_out
    seg_attend = lax.all_gather(attend_out, "tp", axis=1, tiled=True)
    seg_linear = lax.all_gather(linear_out, "tp", axis=1, tiled=True)
    shard_count = seg_attend.shape[1] // head_count
    first_rank = jnp.int32(0) // head_count
    for shard_step in range(shard_count):
        owner_rank = first_rank + shard_step
        rows_attend = lax.dynamic_index_in_dim(attend_view, owner_rank, 1, keepdims=False).reshape(
            -1, out_cols
        )
        rows_linear = lax.dynamic_index_in_dim(linear_view, owner_rank, 1, keepdims=False).reshape(
            -1, out_cols
        )
        part_attend = seg_attend[
            :, shard_step * head_count : (shard_step + 1) * head_count
        ].reshape(tok_rows, -1)
        part_linear = seg_linear[
            :, shard_step * head_count : (shard_step + 1) * head_count
        ].reshape(tok_rows, -1)
        running_out = running_out + jnp.dot(
            part_attend, rows_attend, preferred_element_type=jnp.float32
        )
        running_out = running_out + jnp.dot(
            part_linear, rows_linear, preferred_element_type=jnp.float32
        )
    return running_out.astype(jnp.bfloat16).reshape(1, tok_rows, out_cols)


def solution(mesh):
    in_specs = (
        P(("grp", "fs"), "sp", None),
        P(),
        P(None, ("fs", "tp"), None),
        P(None, ("fs", "tp"), None),
        P(None, ("fs", "tp"), None),
        P(None, ("fs", "tp"), None),
        P(None, ("fs", "tp"), None),
        P(None, ("fs", "tp"), None),
        P(),
        P(),
        P(),
        P(("grp", "fs"), "sp", None),
        P(),
        P(),
        P(),
        P(),
        P(),
        P("grp", ("fs", "tp"), None, None),
        P(None, "tp"),
        P(None, "tp"),
    )
    out_specs = P(("grp", "fs"), "sp", "tp")
    return jax.shard_map(body, mesh=mesh, in_specs=in_specs, out_specs=out_specs, check_vma=False)
```

profile of v0, /device:TPU:11, one launch (start us, length us, event | category | flops | bytes accessed | tf_op | source)
XLA Modules:
  0.0 173.8 jit_solution(11387450350925184077)
XLA Ops:
  6.6 1.3 fusion.46
  7.9 2.0 %fusion.48 = bf16[1,128,2048]{2,1,0:T(8,128)(2,1)} fusion(bf16[1,128,2048]{2,1,0:T(8,128)(2,1)} %param.28, f32[2048]{0:T(1024)} %param.29, f32[128]{0:T(128)S(1)} %add_rsqrt_fusion.4), kind=kLoop, calls=%fused_computation.92 | loop fusion | flops 1048576 | bytes 1057280 | tf_op jit(solution)/shard_map/convert_element_type | solution.py:131
  10.2 1.3 gather_fusion.1
  11.5 1.3 gather_fusion
  12.8 2.4 %bitcast_dynamic-update-slice_fusion.4 = bf16[2048,1792]{1,0:T(8,128)(2,1)} fusion(bf16[256,8,2,128]{3,2,1,0:T(2,128)(2,1)} %bitcast.243), kind=kLoop, calls=%fused_computation.97 | loop fusion | bytes 2097152
  15.2 2.0 %copy.128 = bf16[256,8,2,256]{3,1,2,0:T(8,128)(2,1)S(1)} copy(bf16[256,8,2,256]{3,2,1,0:T(2,128)(2,1)} %bitcast.240) | data formatting | bytes 4194304
  17.2 0.6 gather_fusion.3
  17.8 0.6 gather_fusion.4
  18.4 0.7 gather_fusion.2
  19.1 2.5 %bitcast_dynamic-update-slice_fusion.3 = bf16[2048,1792]{1,0:T(8,128)(2,1)} fusion(bf16[2048,1792]{1,0:T(8,128)(2,1)} %bitcast_dynamic-update-slice_fusion.4, bf16[256,8,2,128]{3,2,1,0:T(2,128)(2,1)} %bitcast.244), kind=kLoop, calls=%fused_computation.96 | loop fusion | bytes 2097152
  21.6 2.4 %bitcast_dynamic-update-slice_fusion.2 = bf16[2048,1792]{1,0:T(8,128)(2,1)} fusion(bf16[2048,1792]{1,0:T(8,128)(2,1)} %bitcast_dynamic-update-slice_fusion.3, bf16[256,8,2,128]{3,2,1,0:T(2,128)(2,1)} %bitcast.245), kind=kLoop, calls=%fused_computation.95 | loop fusion | bytes 2097152
  24.0 2.5 %bitcast_dynamic-update-slice_fusion.1 = bf16[2048,1792]{1,0:T(8,128)(2,1)} fusion(bf16[2048,1792]{1,0:T(8,128)(2,1)} %bitcast_dynamic-update-slice_fusion.2, bf16[256,8,2,128]{3,2,1,0:T(2,128)(2,1)} %bitcast.246), kind=kLoop, calls=%fused_computation.94 | loop fusion | bytes 2097152
  26.6 1.4 fusion.54
  28.0 2.6 %bitcast_dynamic-update-slice_fusion = bf16[2048,1792]{1,0:T(8,128)(2,1)} fusion(bf16[2048,1792]{1,0:T(8,128)(2,1)} %bitcast_dynamic-update-slice_fusion.1, bf16[256,8,2,128]{3,2,1,0:T(2,128)(2,1)} %bitcast.247), kind=kLoop, calls=%fused_computation.93 | loop fusion | bytes 2097152
  30.5 1.5 constant_dynamic-update-slice_fusion
  32.1 1.6 fusion.68
  33.6 6.4 %fusion.37 = bf16[2,128,1792]{2,1,0:T(8,128)(2,1)} fusion(bf16[2,128,2048]{2,1,0:T(8,128)(2,1)} %all-gather.6.cloned.1.call-done, bf16[2048,1792]{1,0:T(8,128)(2,1)} %constant_dynamic-update-slice_fusion), kind=kOutput, calls=%fused_computation.76 | convolution fusion | flops 1879506944 | bytes 9306112 | tf_op jit(solution)/shard_map/std,dp->stp/dot_general | solution.py:138
  40.1 3.8 %all-to-all-start = ((bf16[2,128,1792]{2,1,0:T(8,128)(2,1)}), bf16[2,128,1792]{2,1,0:T(8,128)(2,1)S(1)}, u32[]{:S(2)}, u32[]{:S(2)}) async-start(bf16[2,128,1792]{2,1,0:T(8,128)(2,1)} %fusion.37), calls=%async_computation | async-start | bytes 1835008 | tf_op jit(solution)/shard_map/all_to_all | solution.py:144
  43.9 4.6 %fusion.67 = (bf16[2,1,512,1024]{3,2,1,0:T(8,128)(2,1)}, bf16[2,1,512,1024]{3,2,1,0:T(8,128)(2,1)}) fusion(bf16[2,2,512,1024]{3,2,1,0:T(8,128)(2,1)} %bitcast.227), kind=kLoop, calls=%fused_computation.147 | loop fusion | bytes 8388608 | tf_op jit(solution)/shard_map/jit(dynamic_index_in_dim)/dynamic_slice | solution.py:262
  48.6 5.7 %all-to-all-done = bf16[2,128,1792]{2,1,0:T(8,128)(2,1)S(1)} async-done(((bf16[2,128,1792]{2,1,0:T(8,128)(2,1)}), bf16[2,128,1792]{2,1,0:T(8,128)(2,1)S(1)}, u32[]{:S(2)}, u32[]{:S(2)}) %all-to-all-start) | async-done | bytes 917536 | tf_op jit(solution)/shard_map/all_to_all | solution.py:144
  54.3 4.7 %all-to-all-start.1 = ((f32[2,2,128,256]{3,2,1,0:T(8,128)}), f32[2,2,128,256]{3,2,1,0:T(8,128)S(1)}, u32[]{:S(2)}, u32[]{:S(2)}) async-start(f32[2,2,128,256]{3,2,1,0:T(8,128)} %param.45), calls=%async_computation.1 | async-start | bytes 1048576 | tf_op jit(solution)/shard_map/all_to_all | solution.py:241
  58.9 0.9 fusion.69
  59.9 1.1 copy.83
  61.5 1.2 copy.94
  62.7 1.6 reshape.336
  64.7 9.1 %while.46 = (s32[]{:T(128)}, f32[4,128,256]{2,1,0:T(8,128)S(1)}, f32[4,128]{1,0:T(4,128)S(1)}, f32[2,64,4,256]{3,1,0,2:T(8,128)}, f32[2,64,4,128]{3,2,1,0:T(4,12...) while((s32[]{:T(128)}, f32[4,128,256]{2,1,0:T(8,128)S(1)}, ...), condition=%wide.region_12.13_spmd.clone, body=%wide.region_10.12_spmd.clone.sunk | while | flops 279794688 | bytes 5934213 | solution.py:87
  64.7 0.9 constant_dynamic-slice_fusion.4
  66.3 0.4 convolution_bitcast_fusion.4
  66.7 1.1 fusion.109
  67.9 0.7 convolution_add_fusion.6
  68.6 0.7 fusion.110
  69.3 0.9 constant_dynamic-slice_fusion.4
  70.9 0.4 convolution_bitcast_fusion.4
  71.3 1.1 fusion.109
  72.4 0.7 convolution_add_fusion.6
  73.2 0.7 fusion.110
  73.9 0.8 copy-done.2
  74.8 13.9 %all_gather.28 = bf16[512,4,2,64]{0,3,2,1:T(8,128)(2,1)S(1)} all-gather(bf16[128,4,2,64]{0,3,2,1:T(8,128)(2,1)S(1)} %multiply_convert_fusion.3), channel_id=1, replica_groups=mesh['grp'=2,'sp'=4,'fs'=2,'tp'=2] {'sp'}, dimensions={0}, use_global_device_ids=true | all-gather | bytes 655360 | tf_op jit(solution)/shard_map/all_gather | solution.py:172
  88.8 1.1 copy.84
  90.0 23.7 %all_gather.29 = bf16[512,4,128]{0,2,1:T(8,128)(2,1)S(1)} all-gather(bf16[128,4,128]{0,2,1:T(8,128)(2,1)S(1)} %bitcast.252), channel_id=1, replica_groups=mesh['grp'=2,'sp'=4,'fs'=2,'tp'=2] {'sp'}, dimensions={0}, use_global_device_ids=true | all-gather | bytes 655360 | tf_op jit(solution)/shard_map/all_gather | solution.py:173
  114.1 0.7 multiply_convert_fusion.2
  115.0 3.7 %while.47 = (s32[]{:T(128)}, f32[4,2,128]{2,1,0:T(2,128)S(1)}, f32[4,2,128]{2,1,0:T(2,128)S(1)}, f32[4,2,128,128]{3,2,1,0:T(8,128)S(1)}, s32[2]{0:T(128)S(1)}, /...) while((s32[]{:T(128)}, f32[4,2,128]{2,1,0:T(2,128)S(1)}, ...), condition=%wide.region_8.9_spmd.clone.clone, body=%wide.region_3.8_spmd.clone.clone.sunk | while | flops 102802176 | bytes 4989555 | solution.py:210
  115.0 0.6 dynamic_slice.111
  116.2 1.2 conditional.4
  116.9 0.5 convolution_add_fusion.1
  117.4 0.6 dynamic_slice.111
  119.2 10.2 %all_gather.30 = bf16[128,8,128]{2,0,1:T(8,128)(2,1)S(1)} all-gather(bf16[128,4,128]{2,0,1:T(8,128)(2,1)S(1)} %multiply_convert_fusion.1), channel_id=1, replica_groups=mesh['grp'=2,'sp'=4,'fs'=2,'tp'=2] {'tp'}, dimensions={1}, use_global_device_ids=true | all-gather | bytes 393216 | tf_op jit(solution)/shard_map/all_gather | solution.py:253
  129.5 0.8 copy.113
  130.3 1.0 copy.101
  131.3 0.8 copy.115
  132.0 14.6 %all-gather.2 = f32[4,4,128]{2,1,0:T(4,128)S(1)} all-gather(f32[1,4,128]{2,1,0:T(4,128)S(1)} %bitcast.260), channel_id=2, replica_groups=mesh['grp'=2,'sp'=4,'fs'=2,'tp'=2] {'sp'}, dimensions={0}, use_global_device_ids=true | all-gather | bytes 10240 | tf_op jit(solution)/shard_map/all_gather | solution.py:20
  146.7 1.4 while.45
  146.7 1.3 bitcast_add_fusion.4
  148.2 2.3 %multiply_reduce_fusion = (f32[128,4]{0,1:T(4,128)S(1)}, f32[128,4,256]{0,2,1:T(8,128)S(1)}) fusion(f32[128,4,256]{0,2,1:T(8,128)} %copy.101, f32[4,128,256]{2,1,0:T(8,128)S(1)} %fusion.49, f32[128,4,128]{2,1,0:T(4,128)} %bitcast.257), kind=kOutput, calls=%fused_computation.104 | convolution fusion | flops 201719296 | bytes 1837056 | tf_op jit(solution)/shard_map/jwo,wos->jws/dot_general | solution.py:243
  150.6 0.8 multiply_convert_fusion
  151.4 1.1 copy.102
  152.5 4.8 %all_gather.35 = bf16[128,8,256]{2,0,1:T(8,128)(2,1)S(1)} all-gather(bf16[128,4,256]{2,0,1:T(8,128)(2,1)S(1)} %copy.102), channel_id=1, replica_groups=mesh['grp'=2,'sp'=4,'fs'=2,'tp'=2] {'tp'}, dimensions={1}, use_global_device_ids=true | all-gather | bytes 786432 | tf_op jit(solution)/shard_map/all_gather | solution.py:254
  157.2 0.7 fusion.70
  158.0 1.8 %copy.114 = bf16[128,4,256]{0,2,1:T(8,128)(2,1)} copy(bf16[128,4,256]{2,0,1:T(8,128)(2,1)} %get-tuple-element.513) | data formatting | bytes 524288
  159.8 0.8 copy.116
  160.6 2.2 %fusion.73 = f32[128,1024]{1,0:T(8,128)S(1)} fusion(bf16[128,1024]{0,1:T(8,128)(2,1)} %bitcast.249, bf16[1024,1024]{1,0:T(8,128)(2,1)} %bitcast.225), kind=kOutput, calls=%fused_computation.153 | convolution fusion | flops 268435456 | bytes 2883584 | tf_op jit(solution)/shard_map/dot_general | solution.py:274
  162.8 1.4 fusion.74
  164.2 1.6 convolution_add_fusion.3
  165.9 1.0 fusion.43
  (108 shorter events, 5.0 us)
Async XLA Ops:
  6.5 20.1 %copy-start = (bf16[2048,32]{0,1:T(8,128)(2,1)S(1)}, bf16[2048,32]{0,1:T(8,128)(2,1)}, u32[]{:S(2)}) copy-start(bf16[2048,32]{0,1:T(8,128)(2,1)} %param.36) | copy-start | bytes 393220
  6.5 10.7 %copy-start.10 = (f32[8,128]{1,0:T(8,128)S(1)}, f32[8,128]{1,0:T(8,128)}, u32[]{:S(2)}) copy-start(f32[8,128]{1,0:T(8,128)} %param.38) | copy-start | bytes 12292
  6.5 11.2 %copy-start.1 = (f32[1,128,8]{1,2,0:T(8,128)S(1)}, f32[1,128,8]{1,2,0:T(8,128)}, u32[]{:S(2)}) copy-start(f32[1,128,8]{1,2,0:T(8,128)} %param.39) | copy-start | bytes 12292
  6.5 11.8 %copy-start.7 = (bf16[32,8,128]{2,1,0:T(8,128)(2,1)S(1)}, bf16[32,8,128]{2,1,0:T(8,128)(2,1)}, u32[]{:S(2)}) copy-start(bf16[32,8,128]{2,1,0:T(8,128)(2,1)} %param.37) | copy-start | bytes 196612
  6.5 27.1 %all-gather.6.cloned.1.call-start = ((), (), s32[]{:S(2)}) async-start(), calls=%async_computation.2 | async-start | bytes 1572864 | tf_op jit(solution)/shard_map/all_gather | solution.py:140
  9.9 16.7 %copy-start.6 = (bf16[1,128,2048]{2,1,0:T(8,128)(2,1)S(1)}, bf16[1,128,2048]{2,1,0:T(8,128)(2,1)}, u32[]{:S(2)}) copy-start(bf16[1,128,2048]{2,1,0:T(8,128)(2,1)} %fusion.48) | copy-start | bytes 1572868
  28.0 4.1 %copy-start.5 = (bf16[1024,1024]{1,0:T(8,128)(2,1)S(1)}, bf16[1024,1024]{1,0:T(8,128)(2,1)}, u32[]{:S(2)}) copy-start(bf16[1024,1024]{1,0:T(8,128)(2,1)} %param.46) | copy-start | bytes 6291460
  40.1 14.2 %all-to-all-start = ((bf16[2,128,1792]{2,1,0:T(8,128)(2,1)}), bf16[2,128,1792]{2,1,0:T(8,128)(2,1)S(1)}, u32[]{:S(2)}, u32[]{:S(2)}) async-start(bf16[2,128,1792]{2,1,0:T(8,128)(2,1)} %fusion.37), calls=%async_computation | async-start | bytes 1835008 | tf_op jit(solution)/shard_map/all_to_all | solution.py:144
  54.3 93.8 %all-to-all-start.1 = ((f32[2,2,128,256]{3,2,1,0:T(8,128)}), f32[2,2,128,256]{3,2,1,0:T(8,128)S(1)}, u32[]{:S(2)}, u32[]{:S(2)}) async-start(f32[2,2,128,256]{3,2,1,0:T(8,128)} %param.45), calls=%async_computation.1 | async-start | bytes 1048576 | tf_op jit(solution)/shard_map/all_to_all | solution.py:241
  58.9 87.7 %all-gather.8.cloned.1.call-start = ((), (), s32[]{:S(2)}) async-start(), calls=%async_computation.3 | async-start | bytes 2621440 | tf_op jit(solution)/shard_map/all_gather | solution.py:20
  73.9 0.8 copy-start.2
  114.9 4.1 %copy-start.12 = (f32[128]{0:T(128)S(1)}, f32[128]{0:T(128)}, u32[]{:S(2)}) copy-start(f32[128]{0:T(128)} %param.43) | copy-start | bytes 1540
  115.0 15.3 %copy-start.9 = (f32[2,64,4,256]{3,1,0,2:T(8,128)S(1)}, f32[2,64,4,256]{3,1,0,2:T(8,128)}, u32[]{:S(2)}) copy-start(f32[2,64,4,256]{3,1,0,2:T(8,128)} %get-tuple-element.232) | copy-start | bytes 1572868
  119.2 31.3 %copy-start.11 = (f32[256]{0:T(256)S(1)}, f32[256]{0:T(256)}, u32[]{:S(2)}) copy-start(f32[256]{0:T(256)} %param.44) | copy-start | bytes 3076
  146.7 16.2 %copy-start.3 = (bf16[2,1,512,1024]{3,2,1,0:T(8,128)(2,1)S(1)}, bf16[2,1,512,1024]{3,2,1,0:T(8,128)(2,1)}, u32[]{:S(2)}) copy-start(bf16[2,1,512,1024]{3,2,1,0:T(8,128)(2,1)} %get-tuple-element.506) | copy-start | bytes 6291460
  148.2 17.7 %copy-start.4 = (bf16[2,1,256,1024]{3,2,1,0:T(8,128)(2,1)S(1)}, bf16[2,1,256,1024]{3,2,1,0:T(8,128)(2,1)}, u32[]{:S(2)}) copy-start(bf16[2,1,256,1024]{3,2,1,0:T(8,128)(2,1)} %get-tuple-element.507) | copy-start | bytes 3145732
  160.6 5.3 %copy-start.8 = (bf16[128,4,128]{0,2,1:T(8,128)(2,1)S(1)}, bf16[128,4,128]{0,2,1:T(8,128)(2,1)}, u32[]{:S(2)}) copy-start(bf16[128,4,128]{0,2,1:T(8,128)(2,1)} %copy.115) | copy-start | bytes 393220
Sparse Core Ops, SparseCore 0:
  10.1 21.3 all-gather.5
  74.8 56.7 all-gather.7
where the time goes:
time: 176 us; the launch traced here: 174 us
  blocking collectives  67.2 us (38%)
  local copies, waits for them, and re-layouts  44 us (25%)
  matrix products  22.3 us (13%)
  between operations  13.8 us (8%)
  other arithmetic  10.6 us (6%)
  starting transfers between devices  8.48 us (5%)
  waiting for transfers between devices  5.73 us (3%)
    all_gather x1, blocking collectives, body(): seg_values = lax.all_gather(v_attend, 'sp', axis=0, tiled=True)  23.7 us
    unnamed x37, local copies, waits for them, and re-layouts  19.4 us
    all_gather x1, blocking collectives, entering(): gathered = jax.tree.map(lambda a: lax.all_gather(a, axis), part)  14.6 us
    all_gather x1, blocking collectives, body(): seg_keys = lax.all_gather(k_unit, 'sp', axis=0, tiled=True)  13.9 us
    all_gather x1, blocking collectives, body(): seg_attend = lax.all_gather(attend_out, 'tp', axis=1, tiled=True)  10.2 us
    dot_general x1, matrix products, body(): jnp.einsum('std,dp->stp', lax.all_gather(normed, 'fs', axis=0, tiled=True...  6.43 us
    all_to_all x1, waiting for transfers between devices, body(): lax.all_to_all(computed, 'fs', split_axis=0, concat_axis=2, tiled=True)  5.69 us
    all_gather x1, blocking collectives, body(): seg_linear = lax.all_gather(linear_out, 'tp', axis=1, tiled=True)  4.77 us
  transfers between devices with their start and end apart: 4, of which 1 were waited for; matrix products, arithmetic and copies ran while one was open for 30% of the time, Pallas kernels for 0%

commit v1 on v0

--- a/solution.py
+++ b/solution.py
@@ -1,6 +1,10 @@
+import functools
+
 import jax
 import jax.numpy as jnp
 from jax import lax
+from jax.experimental import pallas as pl
+from jax.experimental.pallas import tpu as pltpu
 from jax.sharding import PartitionSpec as P
 
 MIXER_HEADS = 8
@@ -277,6 +281,372 @@
     return running_out.astype(jnp.bfloat16).reshape(1, tok_rows, out_cols)
 
 
+MESH = pl.DeviceIdType.MESH
+
+
+def group_barrier(n, fs_size, tp_size):
+    z, f, c = lax.axis_index("sp"), lax.axis_index("fs"), lax.axis_index("tp")
+    barrier = pltpu.get_barrier_semaphore()
+    total = n * fs_size * tp_size
+    me = (z * fs_size + f) * tp_size + c
+    for k in range(1, total):
+        other = lax.rem(me + k, total)
+        oz = other // (fs_size * tp_size)
+        of = lax.rem(other // tp_size, fs_size)
+        oc = lax.rem(other, tp_size)
+        pl.semaphore_signal(
+            barrier, inc=1, device_id={"sp": oz, "fs": of, "tp": oc}, device_id_type=MESH
+        )
+    pl.semaphore_wait(barrier, total - 1)
+
+
+def remote(src, dst, send, recv, **where):
+    return pltpu.make_async_remote_copy(
+        src_ref=src,
+        dst_ref=dst,
+        send_sem=send,
+        recv_sem=recv,
+        device_id=where,
+        device_id_type=MESH,
+    )
+
+
+def gather_kernel(
+    n,
+    fs_size,
+    tp_size,
+    hpd,
+    tok_ref,
+    ret_ref,
+    out_ref,
+    rout_ref,
+    recv_a,
+    recv_b,
+    recv_r,
+    send_a,
+    send_up,
+    send_down,
+    send_sib,
+    send_r,
+    loc,
+):
+    z, f, c = lax.axis_index("sp"), lax.axis_index("fs"), lax.axis_index("tp")
+    rows = tok_ref.shape[0]
+    half = rows // tp_size
+    group_barrier(n, fs_size, tp_size)
+    lo = f * hpd
+    hi = lo + hpd - 1
+    near = jnp.minimum(jnp.maximum(z, lo), hi)
+    own = near == z
+
+    def piece(zc):
+        return pl.ds(pl.multiple_of(zc * rows + c * half, half), half)
+
+    mine = pl.ds(pl.multiple_of(c * half, half), half)
+    sends = []
+    for k in range(fs_size):
+        x = lax.rem(f + k, fs_size)
+        copy = remote(
+            tok_ref.at[mine], out_ref.at[piece(z)], send_a.at[k], recv_a.at[z], sp=near, fs=x
+        )
+        if k == 0:
+            pl.when(jnp.logical_not(own))(copy.start)
+        else:
+            copy.start()
+        sends.append(copy)
+    full = pl.ds(pl.multiple_of(z * rows, rows), rows)
+    local = pltpu.make_async_copy(tok_ref, out_ref.at[full], loc.at[0])
+    local_r = pltpu.make_async_copy(ret_ref, rout_ref.at[z], loc.at[1])
+    pl.when(own)(local.start)
+    pl.when(own)(local_r.start)
+    rsends = []
+    for j in range(hpd):
+        for k in range(fs_size):
+            x = lax.rem(f + k, fs_size)
+            there = lo + j
+            copy = remote(
+                ret_ref,
+                rout_ref.at[z],
+                send_r.at[j * fs_size + k],
+                recv_r.at[z],
+                sp=there,
+                fs=x,
+            )
+            go = jnp.logical_not((there == z) & (x == f))
+            pl.when(go)(copy.start)
+            rsends.append((go, copy))
+
+    s = z // hpd
+    mlo = s * hpd
+    mhi = mlo + hpd - 1
+    pending = []
+    for k in range(n):
+        zc = jnp.where(2 * z < n, k, n - 1 - k)
+        here = (zc == z) & (s == f)
+        away = jnp.logical_not(here)
+        block = out_ref.at[piece(zc)]
+        arrive = remote(block, block, send_sib.at[k], recv_a.at[zc], tp=1 - c)
+        pl.when(away)(arrive.wait_recv)
+        pl.when(here)(local.wait)
+        up = remote(block, block, send_up.at[k], recv_a.at[zc], sp=jnp.minimum(z + 1, n - 1))
+        go_up = (zc <= z) & (z + 1 <= mhi)
+        pl.when(go_up)(up.start)
+        down = remote(block, block, send_down.at[k], recv_a.at[zc], sp=jnp.maximum(z - 1, 0))
+        go_down = (zc >= z) & (z - 1 >= mlo)
+        pl.when(go_down)(down.start)
+        sib = remote(block, block, send_sib.at[k], recv_b.at[zc], tp=1 - c)
+        pl.when(away)(sib.start)
+        pending.append((zc, away, sib, go_up, up, go_down, down))
+    pl.when(own)(local_r.wait)
+    for k, copy in enumerate(sends):
+        if k == 0:
+            pl.when(jnp.logical_not(own))(copy.wait_send)
+        else:
+            copy.wait_send()
+    for go, copy in rsends:
+        pl.when(go)(copy.wait_send)
+    for zc, away, sib, go_up, up, go_down, down in pending:
+        pl.when(go_up)(up.wait_send)
+        pl.when(go_down)(down.wait_send)
+        other = out_ref.at[pl.ds(pl.multiple_of(zc * rows + (1 - c) * half, half), half)]
+        came = remote(other, other, send_sib.at[0], recv_b.at[zc], tp=1 - c)
+        pl.when(away)(came.wait_recv)
+        pl.when(away)(sib.wait_send)
+        came_r = remote(ret_ref, rout_ref.at[zc], send_r.at[0], recv_r.at[zc], tp=1 - c)
+        pl.when(away)(came_r.wait_recv)
+
+
+def gather_positions(tokens, retain, n, fs_size, tp_size, hpd):
+    rows, width = tokens.shape
+    dma = pltpu.SemaphoreType.DMA
+    return pl.pallas_call(
+        functools.partial(gather_kernel, n, fs_size, tp_size, hpd),
+        out_shape=(
+            jax.ShapeDtypeStruct((n * rows, width), tokens.dtype),
+            jax.ShapeDtypeStruct((n,) + retain.shape, retain.dtype),
+        ),
+        in_specs=[pl.BlockSpec(memory_space=pltpu.VMEM)] * 2,
+        out_specs=(pl.BlockSpec(memory_space=pl.ANY), pl.BlockSpec(memory_space=pl.ANY)),
+        scratch_shapes=[
+            dma((n,)),
+            dma((n,)),
+            dma((n,)),
+            dma((fs_size,)),
+            dma((n,)),
+            dma((n,)),
+            dma((n,)),
+            dma((hpd * fs_size,)),
+            dma((2,)),
+        ],
+        compiler_params=pltpu.CompilerParams(collective_id=0, has_side_effects=True),
+    )(tokens, retain)
+
+
+def exchange_kernel(
+    n,
+    fs_size,
+    tp_size,
+    hpd,
+    mix_ref,
+    out_ref,
+    stage,
+    recv_row,
+    recv_x,
+    recv_s,
+    send_row,
+    send_x,
+    send_s,
+    loc,
+):
+    z, f, c = lax.axis_index("sp"), lax.axis_index("fs"), lax.axis_index("tp")
+    rows = out_ref.shape[1]
+    group_barrier(n, fs_size, tp_size)
+    s = z // hpd
+    keep = s == f
+    cross = jnp.logical_not(keep)
+
+    def head(x, core, zs):
+        return (x * tp_size + core) * hpd + lax.rem(zs, hpd)
+
+    def chunk(zt):
+        return mix_ref.at[pl.ds(pl.multiple_of(zt * rows, rows), rows)]
+
+    my_head = head(f, c, z)
+    waits = []
+    for k in range(1, n):
+        zt = lax.rem(z + k, n)
+        kept = remote(chunk(zt), out_ref.at[my_head], send_row.at[k], recv_row.at[z], sp=zt)
+        moved = remote(chunk(zt), stage.at[z], send_row.at[k], recv_row.at[z], sp=zt)
+        pl.when(keep)(kept.start)
+        pl.when(cross)(moved.start)
+        waits.append((None, kept))
+    local = pltpu.make_async_copy(chunk(z), out_ref.at[my_head], loc)
+    pl.when(keep)(local.start)
+    sib0 = remote(chunk(z), out_ref.at[my_head], send_s.at[my_head], recv_s.at[my_head], tp=1 - c)
+    pl.when(keep)(sib0.start)
+    waits.append((keep, sib0))
+    x0 = remote(chunk(z), out_ref.at[my_head], send_x.at[0], recv_x.at[my_head], fs=s)
+    pl.when(cross)(x0.start)
+    waits.append((cross, x0))
+    for k in range(1, n):
+        zs = lax.rem(z + k, n)
+        sq = zs // hpd
+        hd = head(f, c, zs)
+        final = sq == f
+        onward = jnp.logical_not(final)
+        landed = remote(stage.at[zs], stage.at[zs], send_x.at[k], recv_row.at[zs], tp=1 - c)
+        landed.wait_recv()
+        sib = remote(out_ref.at[hd], out_ref.at[hd], send_s.at[hd], recv_s.at[hd], tp=1 - c)
+        pl.when(final)(sib.start)
+        waits.append((final, sib))
+        xs = remote(stage.at[zs], out_ref.at[hd], send_x.at[k], recv_x.at[hd], fs=sq)
+        pl.when(onward)(xs.start)
+        waits.append((onward, xs))
+    for k in range(1, fs_size):
+        x = lax.rem(f + k, fs_size)
+        for j in range(hpd):
+            hd = head(x, c, j)
+            block = out_ref.at[hd]
+            came = remote(block, block, send_s.at[hd], recv_x.at[hd], tp=1 - c)
+            came.wait_recv()
+            sib = remote(block, block, send_s.at[hd], recv_s.at[hd], tp=1 - c)
+            sib.start()
+            waits.append((None, sib))
+    for x in range(fs_size):
+        for j in range(hpd):
+            hd = head(x, 1 - c, j)
+            block = out_ref.at[hd]
+            remote(block, block, send_s.at[hd], recv_s.at[hd], tp=1 - c).wait_recv()
+    pl.when(keep)(local.wait)
+    for go, copy in waits:
+        if go is None:
+            copy.wait_send()
+        else:
+            pl.when(go)(copy.wait_send)
+
+
+def exchange_heads(mixed, n, fs_size, tp_size, hpd):
+    rows, width = mixed.shape[0] // n, mixed.shape[1]
+    heads = fs_size * tp_size * hpd
+    dma = pltpu.SemaphoreType.DMA
+    return pl.pallas_call(
+        functools.partial(exchange_kernel, n, fs_size, tp_size, hpd),
+        out_shape=jax.ShapeDtypeStruct((heads, rows, width), mixed.dtype),
+        in_specs=[pl.BlockSpec(memory_space=pltpu.VMEM)],
+        out_specs=pl.BlockSpec(memory_space=pl.ANY),
+        scratch_shapes=[
+            pltpu.VMEM((n, rows, width), mixed.dtype),
+            dma((n,)),
+            dma((heads,)),
+            dma((heads,)),
+            dma((n,)),
+            dma((n,)),
+            dma((heads,)),
+            dma,
+        ],
+        compiler_params=pltpu.CompilerParams(collective_id=1, has_side_effects=True),
+    )(mixed)
+
+
+def pair_body(
+    tokens,
+    norm_gain,
+    query_attend,
+    key_attend,
+    value_attend,
+    query_linear,
+    key_linear,
+    value_linear,
+    decay_down,
+    decay_up,
+    decay_bias,
+    log_retain,
+    query_gain,
+    key_gain,
+    diff_lambda,
+    mix_gain,
+    state_gain,
+    init_state,
+    output_attend,
+    output_linear,
+):
+    n, fs_size, tp_size = lax.axis_size("sp"), lax.axis_size("fs"), lax.axis_size("tp")
+    hpd = query_attend.shape[1]
+    z = lax.axis_index("sp")
+    slot = lax.rem(z, hpd)
+    seq = z // hpd
+    head = (lax.axis_index("fs") * tp_size + lax.axis_index("tp")) * hpd + slot
+    rows = tokens.shape[1]
+    positions, retained = gather_positions(
+        tokens[0], jnp.transpose(log_retain[0]), n, fs_size, tp_size, hpd
+    )
+    retain = lax.dynamic_index_in_dim(retained, head, 1, False).reshape(n * rows)
+    normed = rms_scale(positions, norm_gain).astype(jnp.bfloat16)
+
+    def project(weight):
+        return jnp.dot(
+            normed,
+            lax.dynamic_index_in_dim(weight, slot, 1, False),
+            preferred_element_type=jnp.float32,
+        ).astype(jnp.bfloat16)
+
+    length = n * rows
+    q_unit = rms_scale(project(query_attend).reshape(length, 2, HD_A), query_gain)
+    k_unit = rms_scale(
+        project(key_attend).reshape(length, 2, HD_A), lax.dynamic_index_in_dim(key_gain, head, 0, False)
+    )
+    v_attend = project(value_attend)
+    scores = jnp.einsum(
+        "qmd,kmd->mqk",
+        q_unit.astype(jnp.bfloat16),
+        k_unit.astype(jnp.bfloat16),
+        preferred_element_type=jnp.float32,
+    ) * HD_A ** (-0.5)
+    blocks = jnp.arange(length, dtype=jnp.int32) // BLK
+    scores = jnp.where(blocks[:, None] >= blocks[None, :], scores, -jnp.inf)
+    raised = jnp.exp(scores - jnp.max(scores, axis=-1, keepdims=True))
+    totals = jnp.sum(raised, axis=-1, keepdims=True)
+    sums = jnp.einsum(
+        "mqk,kv->mqv", raised.astype(jnp.bfloat16), v_attend, preferred_element_type=jnp.float32
+    )
+    lam = lax.dynamic_index_in_dim(diff_lambda, head, 0, False)
+    diff_raw = sums[0] / totals[0] - lam * sums[1] / totals[1]
+    attend_out = rms_scale(diff_raw, mix_gain).astype(jnp.bfloat16)
+    low_rank = jnp.dot(normed, decay_down, preferred_element_type=jnp.float32).astype(jnp.bfloat16)
+    pre_act = jnp.dot(
+        low_rank,
+        lax.dynamic_index_in_dim(decay_up, head, 1, False),
+        preferred_element_type=jnp.float32,
+    ) + lax.dynamic_index_in_dim(decay_bias, head, 0, False)
+    log_decay = jax.nn.log_sigmoid(pre_act) / decay_tau + retain[:, None]
+    start = lax.dynamic_index_in_dim(
+        lax.dynamic_index_in_dim(init_state, seq, 0, False), slot, 0, False
+    )
+    _, _, inside, reaching = linear_blocks(
+        project(query_linear).astype(jnp.float32)[:, None] * HDK ** (-0.5),
+        project(key_linear).astype(jnp.float32)[:, None],
+        project(value_linear).astype(jnp.float32)[:, None],
+        log_decay[:, None],
+    )
+    linear_raw = inside[:, 0] + jnp.dot(reaching[:, 0], start, precision=lax.Precision.HIGHEST)
+    linear_out = rms_scale(linear_raw, state_gain).astype(jnp.bfloat16)
+    mixed = jnp.concatenate([attend_out, linear_out], axis=1)
+    arrived = exchange_heads(mixed, n, fs_size, tp_size, hpd)
+    heads = arrived.shape[0]
+    out = jnp.einsum(
+        "htw,hwo->to",
+        arrived[:, :, :DV_A],
+        output_attend.reshape(heads, DV_A, -1),
+        preferred_element_type=jnp.float32,
+    ) + jnp.einsum(
+        "htw,hwo->to",
+        arrived[:, :, DV_A:],
+        output_linear.reshape(heads, HDV, -1),
+        preferred_element_type=jnp.float32,
+    )
+    return out.astype(jnp.bfloat16)[None]
+
+
 def solution(mesh):
     in_specs = (
         P(("grp", "fs"), "sp", None),
@@ -301,4 +671,7 @@
         P(None, "tp"),
     )
     out_specs = P(("grp", "fs"), "sp", "tp")
-    return jax.shard_map(body, mesh=mesh, in_specs=in_specs, out_specs=out_specs, check_vma=False)
+    fs_size, tp_size, sp_size = mesh.shape["fs"], mesh.shape["tp"], mesh.shape["sp"]
+    pairs = MIXER_HEADS // tp_size
+    chosen = pair_body if pairs == sp_size and tp_size == 2 else body
+    return jax.shard_map(chosen, mesh=mesh, in_specs=in_specs, out_specs=out_specs, check_vma=False)

time: 176 us -> 138 us (0.78)
  blocking collectives: 67.2 us -> 0 us
  Pallas kernels: 0 us -> 65.5 us
  local copies, waits for them, and re-layouts: 44 us -> 21.8 us
  between operations: 13.8 us -> 0.35 us
  matrix products: 22.3 us -> 35 us
  starting transfers between devices: 8.48 us -> 0 us
  waiting for transfers between devices: 5.73 us -> 0 us
  other arithmetic: 10.6 us -> 14 us
    all_gather x5 -> x0, blocking collectives: 67.2 us -> none  [the longest x1 23.7 us: body(): seg_values = lax.all_gather(v_attend, 'sp', axis=0, tiled=True)]
    pallas_call x0 -> x2, Pallas kernels: none -> 65.5 us  [the longest x1 40.8 us: gather_positions(): pl.pallas_call(functools.partial(gather_kernel, n, fs_size, tp_size, hpd)...]
    unnamed x37 -> x30, local copies, waits for them, and re-layouts: 19.4 us -> 1.9 us
    all_to_all x2 -> x0, starting transfers between devices: 8.45 us -> none  [the longest x1 4.65 us: body(): lax.all_to_all(init_state, 'fs', split_axis=0, concat_axis=1, tiled=True)[0]]
    convert_element_type x7 -> x0, local copies, waits for them, and re-layouts: 6.46 us -> none  [the longest x2 2.76 us: body(): v_lin.astype(jnp.float32)]
    all_to_all x2 -> x0, waiting for transfers between devices: 5.69 us -> none  [the longest x1 5.69 us: body(): lax.all_to_all(computed, 'fs', split_axis=0, concat_axis=2, tiled=True)]
    dot_general x9 -> x11, matrix products: 17.2 us -> 22.1 us  [the longest x5 4.52 us: project(): jnp.dot(normed, lax.dynamic_index_in_dim(weight, slot, 1, False), preferr...]
    dynamic_slice x4 -> x7, local copies, waits for them, and re-layouts: 7.4 us -> 12.3 us  [the longest x4 10.1 us: project(): lax.dynamic_index_in_dim(weight, slot, 1, False)]
  transfers between devices with their start and end apart: 4 -> 0, of which waited for: 1 -> 0; matrix products, arithmetic and copies ran while one was open for 30% -> 0% of each run, Pallas kernels for 0% -> 0%
where the time goes in v1:
time: 138 us; the launch traced here: 137 us
  Pallas kernels  65.5 us (47%)
  matrix products  35 us (25%)
  local copies, waits for them, and re-layouts  21.8 us (16%)
  other arithmetic  14 us (10%)
    pallas_call x1, Pallas kernels, gather_positions(): pl.pallas_call(functools.partial(gather_kernel, n, fs_size, tp_size, hpd)...  40.8 us
    pallas_call x1, Pallas kernels, exchange_heads(): pl.pallas_call(functools.partial(exchange_kernel, n, fs_size, tp_size, hp...  24.7 us
    dynamic_slice x4, local copies, waits for them, and re-layouts, project(): lax.dynamic_index_in_dim(weight, slot, 1, False)  10.1 us
    dot_general x8, matrix products, advance(): jnp.einsum('jwo,wos->jws', question_patch_lines * jnp.exp(running_state),...  6.71 us
    dynamic_slice x8, local copies, waits for them, and re-layouts, linear_blocks(): lax.scan(advance, start_carry, (split_blocks(queries), split_blocks(keys_...  6.13 us
    dynamic_update_slice x8, other arithmetic, linear_blocks(): lax.scan(advance, start_carry, (split_blocks(queries), split_blocks(keys_...  5.02 us
    dot_general x5, matrix products, project(): jnp.dot(normed, lax.dynamic_index_in_dim(weight, slot, 1, False), preferr...  4.52 us
    dot_general x1, matrix products, pair_body(): jnp.einsum('mqk,kv->mqv', raised.astype(jnp.bfloat16), v_attend, preferre...  4.45 us

profile of v1, /device:TPU:11, one launch (start us, length us, event | category | flops | bytes accessed | tf_op | source)
XLA Modules:
  0.0 137.0 jit_solution(10662319752780858699)
XLA Ops:
  0.0 4.3 %constant_dynamic-slice_fusion.7 = (bf16[2048,1,128]{2,1,0:T(2,128)(2,1)}, bf16[2048,1,128]{2,1,0:T(2,128)(2,1)S(1)}) fusion(bf16[2048,2,128]{2,1,0:T(2,128)(2,1)} %param.26, s32[]{:T(128)S(6)} %select_n.65, bf16[2048,2,128]{2,1,0:T(2,128)(2,1)} %param.25), kind=kLoop, calls=%fused_computation.141 | loop fusion | bytes 2097156 | tf_op jit(solution)/shard_map/jit(dynamic_index_in_dim)/dynamic_slice | solution.py:589
  4.4 40.8 %shard_map.190 = (bf16[512,2048]{1,0:T(8,128)(2,1)}, f32[4,8,128]{2,1,0:T(8,128)}) custom-call(bf16[128,2048]{1,0:T(8,128)(2,1)} %bitcast.213, f32[8,128]{1,0:T(8,128)} %bitcast.222), custom_call_target="tpu_custom_call" | custom-call | tf_op jit(solution)/shard_map/pallas_call | solution.py:422
  45.1 2.2 %fusion.44 = f32[512]{0:T(512)S(1)} fusion(bf16[512,2048]{1,0:T(8,128)(2,1)} %get-tuple-element.60), kind=kLoop, calls=%fused_computation.55 | loop fusion | flops 3145216 | bytes 2099200 | tf_op jit(solution)/shard_map/reduce_sum | solution.py:38
  47.4 0.5 fusion.46
  47.9 0.9 fusion.67
  48.8 1.1 copy-done.9
  49.9 1.1 constant_dynamic-slice_fusion.10
  51.1 1.5 %fusion.64 = (f32[512,2]{0,1:T(2,128)S(1)}, bf16[512,128]{0,1:T(8,128)(2,1)}) fusion(bf16[512,2048]{1,0:T(8,128)(2,1)S(1)} %fusion.46, bf16[2048,1,128]{2,1,0:T(2,128)(2,1)S(1)} %constant_dynamic-slice_fusion.10), kind=kOutput, calls=%fused_computation.102 | convolution fusion | flops 268696576 | bytes 2756608 | tf_op jit(solution)/shard_map/dot_general | solution.py:587
  52.6 0.8 fusion.91
  53.4 0.2 broadcast_compare_fusion
  53.6 2.9 %fusion.47 = (f32[2,512]{1,0:T(2,128)S(1)}, f32[2,512,512]{1,2,0:T(8,128)}) fusion(pred[512,512]{0,1:T(8,128)(4,1)S(1)} %broadcast_compare_fusion, bf16[512,2,64]{0,2,1:T(8,128)(2,1)S(1)} %bitcast.217, f32[2,64]{1,0:T(2,128)S(1)} %fusion.91, f32[512,2]{0,1:T(2,128)S(1)} %add_rsqrt_fusion, bf16[512,2,64]{0,2,1:T(8,128)(2,1)} %bitcast.218, ...), kind=kOutput, calls=%fused_computation.60 | convolution fusion | flops 69204992 | bytes 2634496 | tf_op jit(solution)/shard_map/qmd,kmd->mqk/dot_general | solution.py:599
  56.5 4.4 %fusion.57 = f32[2,512,128]{2,1,0:T(8,128)} fusion(f32[2,512,512]{1,2,0:T(8,128)} %get-tuple-element.145, f32[2,512]{1,0:T(2,128)S(1)} %get-tuple-element.144, pred[512,512]{0,1:T(8,128)(4,1)S(1)} %broadcast_compare_fusion, bf16[512,2048]{1,0:T(8,128)(2,1)} %copy-done.1, bf16[2048,1,128]{2,1,0:T(2,128)(2,1)S(1)} %copy-done.8), kind=kOutput, calls=%fused_computation.81 | convolution fusion | flops 404815872 | bytes 5509120 | tf_op jit(solution)/shard_map/mqk,kv->mqv/dot_general | solution.py:609
  61.0 2.2 %fusion.48 = f32[2,512]{1,0:T(2,128)S(1)} fusion(f32[2,512,512]{1,2,0:T(8,128)} %get-tuple-element.145, f32[2,512]{1,0:T(2,128)S(1)} %get-tuple-element.144, pred[512,512]{0,1:T(8,128)(4,1)S(1)} %broadcast_compare_fusion), kind=kLoop, calls=%fused_computation.61 | loop fusion | flops 2096128 | bytes 2367488 | tf_op jit(solution)/shard_map/reduce_sum | solution.py:608
  63.2 0.6 dynamic_slice.64
  63.8 2.0 %multiply_reduce_fusion.1 = (f32[512]{0:T(512)S(1)}, f32[512,128]{1,0:T(8,128)S(1)}) fusion(f32[512]{0:T(512)S(1)} %bitcast.221, f32[2,512,128]{2,1,0:T(8,128)} %fusion.57, f32[]{:T(128)} %bitcast.14, f32[512]{0:T(512)S(1)} %bitcast.220), kind=kLoop, calls=%fused_computation.119 | loop fusion | flops 392704 | bytes 792580 | tf_op jit(solution)/shard_map/reduce_sum | solution.py:38
  66.0 2.3 %constant_dynamic-slice_fusion.2 = bf16[2048,1,256]{2,1,0:T(2,128)(2,1)S(1)} fusion(bf16[2048,2,256]{2,1,0:T(2,128)(2,1)S(1)} %copy-done.5, s32[]{:T(128)S(6)} %select_n.65), kind=kLoop, calls=%fused_computation.136 | loop fusion | bytes 2097156 | tf_op jit(solution)/shard_map/jit(dynamic_index_in_dim)/dynamic_slice | solution.py:589
  68.3 0.7 convolution_convert_fusion
  69.0 0.4 copy-done.6
  69.5 0.3 copy-done.7
  69.8 2.4 %constant_dynamic-slice_fusion.1 = (bf16[2048,1,128]{2,1,0:T(2,128)(2,1)S(1)}, bf16[2048,1,128]{2,1,0:T(2,128)(2,1)S(1)}) fusion(bf16[2048,2,128]{2,1,0:T(2,128)(2,1)S(1)} %copy-done.6, s32[]{:T(128)S(6)} %select_n.65, bf16[2048,2,128]{2,1,0:T(2,128)(2,1)S(1)} %copy-done.7), kind=kLoop, calls=%fused_computation.135 | loop fusion | bytes 2097156 | tf_op jit(solution)/shard_map/jit(dynamic_index_in_dim)/dynamic_slice | solution.py:589
  72.2 0.7 convolution_convert_fusion.2
  72.9 0.7 fusion.55
  73.6 0.7 constant_dynamic-slice_fusion.4
  74.3 0.9 constant_dynamic-slice_fusion.6
  75.2 0.7 fusion.92
  75.9 3.2 %fusion.72 = f32[512,128]{1,0:T(8,128)} fusion(bf16[512,2048]{1,0:T(8,128)(2,1)} %copy-done.1, bf16[2048,32]{0,1:T(8,128)(2,1)} %param.30, f32[512]{0:T(512)S(1)} %bitcast.223, f32[128]{0:T(128)S(1)} %fusion.92, bf16[32,1,128]{2,1,0:T(2,128)(2,1)S(1)} %constant_dynamic-slice_fusion.6), kind=kOutput, calls=%fused_computation.110 | convolution fusion | flops 72040448 | bytes 2501120 | tf_op jit(solution)/shard_map/dot_general | solution.py:616
  79.1 25.1 %while.17 = (s32[]{:T(128)}, f32[1,128,256]{2,1,0:T(8,128)S(1)}, f32[1,128]{1,0:T(1,128)S(1)}, f32[8,64,1,256]{3,1,2,0:T(8,128)}, f32[8,64,1,128]{3,1,2,0:T(8,12...) while((s32[]{:T(128)}, f32[1,128,256]{2,1,0:T(8,128)S(1)}, ...), condition=%wide.region_8.9_spmd.clone, body=%wide.region_6.8_spmd.clone.sunk | while | flops 69951744 | bytes 1272961 | solution.py:91
  79.1 0.8 constant_dynamic-slice_fusion.12
  80.4 0.8 fusion.140
  81.2 0.6 multiply_dynamic-update-slice_fusion.2
  81.9 0.4 fusion.137
  82.3 0.8 constant_dynamic-slice_fusion.12
  83.5 0.8 fusion.140
  84.4 0.6 multiply_dynamic-update-slice_fusion.2
  85.0 0.4 fusion.137
  85.4 0.8 constant_dynamic-slice_fusion.12
  86.7 0.8 fusion.140
  87.5 0.6 multiply_dynamic-update-slice_fusion.2
  88.1 0.4 fusion.137
  88.5 0.8 constant_dynamic-slice_fusion.12
  89.8 0.8 fusion.140
  90.6 0.6 multiply_dynamic-update-slice_fusion.2
  91.3 0.4 fusion.137
  91.7 0.8 constant_dynamic-slice_fusion.12
  92.9 0.8 fusion.140
  93.8 0.6 multiply_dynamic-update-slice_fusion.2
  94.4 0.4 fusion.137
  94.8 0.8 constant_dynamic-slice_fusion.12
  96.1 0.8 fusion.140
  96.9 0.6 multiply_dynamic-update-slice_fusion.2
  97.6 0.4 fusion.137
  98.0 0.8 constant_dynamic-slice_fusion.12
  99.2 0.8 fusion.140
  100.1 0.6 multiply_dynamic-update-slice_fusion.2
  100.7 0.4 fusion.137
  101.1 0.8 constant_dynamic-slice_fusion.12
  102.4 0.8 fusion.140
  103.2 0.6 multiply_dynamic-update-slice_fusion.2
  103.8 0.4 fusion.137
  104.3 1.9 %multiply_reduce_fusion = (f32[512]{0:T(512)S(1)}, f32[512,256]{1,0:T(8,128)S(1)}) fusion(f32[512,256]{1,0:T(8,128)} %bitcast.212, f32[512,128]{1,0:T(8,128)} %bitcast.214, f32[2,2,128,256]{3,2,1,0:T(8,128)} %param.39, s32[]{:T(128)S(6)} %select_n.71, s32[]{:T(128)S(6)} %select_n.72), kind=kOutput, calls=%fused_computation.95 | convolution fusion | flops 201719296 | bytes 1443848 | tf_op jit(solution)/shard_map/dot_general | solution.py:631
  106.3 0.8 pad_maximum_fusion.mix_ref
  107.1 24.7 %shard_map.191 = bf16[8,128,384]{2,1,0:T(8,128)(2,1)} custom-call(bf16[512,384]{1,0:T(8,128)(2,1)} %pad_maximum_fusion.mix_ref), custom_call_target="tpu_custom_call" | custom-call | tf_op jit(solution)/shard_map/pallas_call | solution.py:532
  131.8 1.5 %convolution_bitcast_fusion.2 = f32[128,1024]{1,0:T(8,128)S(1)} fusion(bf16[8,128,1024]{2,1,0:T(8,128)(2,1)S(1)} %bitcast.204, bf16[8,128,384]{2,1,0:T(8,128)(2,1)} %shard_map.191), kind=kOutput, calls=%fused_computation.63 | convolution fusion | flops 268435456 | bytes 2883584 | tf_op jit(solution)/shard_map/htw,hwo->to/dot_general | solution.py:636
  133.3 3.7 %fusion.52 = bf16[1,128,1024]{2,1,0:T(8,128)(2,1)} fusion(f32[128,1024]{1,0:T(8,128)S(1)} %convolution_bitcast_fusion.2, bf16[8,256,1024]{2,1,0:T(8,128)(2,1)} %bitcast.209, bf16[8,128,384]{2,1,0:T(8,128)(2,1)S(1)} %copy-done.4), kind=kOutput, calls=%fused_computation.69 | convolution fusion | flops 537133056 | bytes 5505024 | tf_op jit(solution)/shard_map/htw,hwo->to/dot_general | solution.py:641
  (90 shorter events, 4.3 us)
Async XLA Ops:
  0.0 131.8 %copy-start = (bf16[1024,1024]{1,0:T(8,128)(2,1)S(1)}, bf16[1024,1024]{1,0:T(8,128)(2,1)}, u32[]{:S(2)}) copy-start(bf16[1024,1024]{1,0:T(8,128)(2,1)} %param.40) | copy-start | bytes 6291460
  4.3 43.0 %copy-start.10 = (f32[2048]{0:T(1024)S(1)}, f32[2048]{0:T(1024)}, u32[]{:S(2)}) copy-start(f32[2048]{0:T(1024)} %param.23) | copy-start | bytes 24580
  45.1 2.3 %copy-start.3 = (bf16[512,2048]{1,0:T(8,128)(2,1)S(1)}, bf16[512,2048]{1,0:T(8,128)(2,1)}, u32[]{:S(2)}) copy-start(bf16[512,2048]{1,0:T(8,128)(2,1)} %get-tuple-element.60) | copy-start | bytes 6291460
  47.9 3.1 %copy-start.1 = (bf16[512,2048]{1,0:T(8,128)(2,1)}, bf16[512,2048]{1,0:T(8,128)(2,1)S(1)}, u32[]{:S(2)}) copy-start(bf16[512,2048]{1,0:T(8,128)(2,1)S(1)} %fusion.46) | copy-start | bytes 6291460
  47.9 2.0 %copy-start.9 = (bf16[2048,2,128]{2,1,0:T(2,128)(2,1)S(1)}, bf16[2048,2,128]{2,1,0:T(2,128)(2,1)}, u32[]{:S(2)}) copy-start(bf16[2048,2,128]{2,1,0:T(2,128)(2,1)} %param.24) | copy-start | bytes 3145732
  49.9 3.7 %copy-start.13 = (f32[64]{0:T(128)S(1)}, f32[64]{0:T(128)}, u32[]{:S(2)}) copy-start(f32[64]{0:T(128)} %param.34) | copy-start | bytes 772
  52.6 3.9 %copy-start.8 = (bf16[2048,1,128]{2,1,0:T(2,128)(2,1)S(1)}, bf16[2048,1,128]{2,1,0:T(2,128)(2,1)}, u32[]{:S(2)}) copy-start(bf16[2048,1,128]{2,1,0:T(2,128)(2,1)} %get-tuple-element.150) | copy-start | bytes 1572868
  61.0 2.3 %copy-start.14 = (f32[8]{0:T(128)S(1)}, f32[8]{0:T(128)}, u32[]{:S(2)}) copy-start(f32[8]{0:T(128)} %param.36) | copy-start | bytes 100
  61.0 4.8 %copy-start.12 = (f32[128]{0:T(128)S(1)}, f32[128]{0:T(128)}, u32[]{:S(2)}) copy-start(f32[128]{0:T(128)} %param.37) | copy-start | bytes 1540
  61.0 5.0 %copy-start.5 = (bf16[2048,2,256]{2,1,0:T(2,128)(2,1)S(1)}, bf16[2048,2,256]{2,1,0:T(2,128)(2,1)}, u32[]{:S(2)}) copy-start(bf16[2048,2,256]{2,1,0:T(2,128)(2,1)} %param.29) | copy-start | bytes 6291460
  66.0 2.3 %copy-start.2 = (bf16[512,2048]{1,0:T(8,128)(2,1)S(1)}, bf16[512,2048]{1,0:T(8,128)(2,1)}, u32[]{:S(2)}) copy-start(bf16[512,2048]{1,0:T(8,128)(2,1)} %copy-done.1) | copy-start | bytes 6291460
  68.2 1.2 copy-start.6
  68.2 1.5 %copy-start.7 = (bf16[2048,2,128]{2,1,0:T(2,128)(2,1)S(1)}, bf16[2048,2,128]{2,1,0:T(2,128)(2,1)}, u32[]{:S(2)}) copy-start(bf16[2048,2,128]{2,1,0:T(2,128)(2,1)} %param.28) | copy-start | bytes 3145732
  79.1 27.0 %copy-start.11 = (f32[256]{0:T(256)S(1)}, f32[256]{0:T(256)}, u32[]{:S(2)}) copy-start(f32[256]{0:T(256)} %param.38) | copy-start | bytes 3076
  131.8 1.5 %copy-start.4 = (bf16[8,128,384]{2,1,0:T(8,128)(2,1)S(1)}, bf16[8,128,384]{2,1,0:T(8,128)(2,1)}, u32[]{:S(2)}) copy-start(bf16[8,128,384]{2,1,0:T(8,128)(2,1)} %shard_map.191) | copy-start | bytes 2359300

commit v2 on v1

--- a/solution.py
+++ b/solution.py
@@ -318,8 +318,21 @@
     hpd,
     tok_ref,
     ret_ref,
-    out_ref,
+    gain_ref,
+    down_ref,
+    wq_ref,
+    wk_ref,
+    wv_ref,
+    lq_ref,
+    lk_ref,
+    lv_ref,
+    proj_ref,
+    low_ref,
     rout_ref,
+    seq_ref,
+    raw_ref,
+    raw_v_ref,
+    w_ref,
     recv_a,
     recv_b,
     recv_r,
@@ -329,10 +342,18 @@
     send_sib,
     send_r,
     loc,
+    wsem,
 ):
     z, f, c = lax.axis_index("sp"), lax.axis_index("fs"), lax.axis_index("tp")
-    rows = tok_ref.shape[0]
+    rows, width = tok_ref.shape
     half = rows // tp_size
+    loads = [
+        pltpu.make_async_copy(ref, raw_ref.at[i], wsem.at[i])
+        for i, ref in enumerate((wq_ref, wk_ref, wv_ref, lq_ref, lk_ref))
+    ]
+    loads.append(pltpu.make_async_copy(lv_ref, raw_v_ref, wsem.at[5]))
+    for load in loads:
+        load.start()
     group_barrier(n, fs_size, tp_size)
     lo = f * hpd
     hi = lo + hpd - 1
@@ -347,7 +368,7 @@
     for k in range(fs_size):
         x = lax.rem(f + k, fs_size)
         copy = remote(
-            tok_ref.at[mine], out_ref.at[piece(z)], send_a.at[k], recv_a.at[z], sp=near, fs=x
+            tok_ref.at[mine], seq_ref.at[piece(z)], send_a.at[k], recv_a.at[z], sp=near, fs=x
         )
         if k == 0:
             pl.when(jnp.logical_not(own))(copy.start)
@@ -355,7 +376,7 @@
             copy.start()
         sends.append(copy)
     full = pl.ds(pl.multiple_of(z * rows, rows), rows)
-    local = pltpu.make_async_copy(tok_ref, out_ref.at[full], loc.at[0])
+    local = pltpu.make_async_copy(tok_ref, seq_ref.at[full], loc.at[0])
     local_r = pltpu.make_async_copy(ret_ref, rout_ref.at[z], loc.at[1])
     pl.when(own)(local.start)
     pl.when(own)(local_r.start)
@@ -376,15 +397,62 @@
             pl.when(go)(copy.start)
             rsends.append((go, copy))
 
+    slot = lax.rem(z, hpd)
+    step = 128
+
+    def pick(source, target_cols, parts, part):
+        span = step * parts * hpd
+        sel = (
+            lax.broadcasted_iota(jnp.int32, (step, span), 1)
+            == (lax.broadcasted_iota(jnp.int32, (step, span), 0) * parts + part) * hpd + slot
+        ).astype(jnp.bfloat16)
+
+        def one(i, carry):
+            block = source[pl.ds(pl.multiple_of(i * span, span), span), :]
+            w_ref[pl.ds(pl.multiple_of(i * step, step), step), target_cols] = jnp.dot(
+                sel, block, preferred_element_type=jnp.float32
+            ).astype(jnp.bfloat16)
+            return carry
+
+        lax.fori_loop(0, width // step, one, 0)
+
+    for i in range(5):
+        loads[i].wait()
+        pick(raw_ref.at[i], slice(i * 128, (i + 1) * 128), 1, 0)
+    loads[5].wait()
+    for part in range(2):
+        pick(raw_v_ref, slice((5 + part) * 128, (6 + part) * 128), 2, part)
+
     s = z // hpd
     mlo = s * hpd
     mhi = mlo + hpd - 1
     pending = []
+
+    def order(k):
+        return jnp.where(2 * z < n, k, n - 1 - k)
+
+    def finish(k):
+        zc = order(k)
+        away = jnp.logical_not((zc == z) & (s == f))
+        other = seq_ref.at[pl.ds(pl.multiple_of(zc * rows + (1 - c) * half, half), half)]
+        came = remote(other, other, send_sib.at[0], recv_b.at[zc], tp=1 - c)
+        pl.when(away)(came.wait_recv)
+        at = pl.ds(pl.multiple_of(zc * rows, rows), rows)
+        x = seq_ref[at, :].astype(jnp.float32)
+        scale = lax.rsqrt(jnp.mean(x * x, axis=-1, keepdims=True) + norm_eps)
+        normed = (x * scale * gain_ref[...]).astype(jnp.bfloat16)
+        proj_ref[at, :] = jnp.dot(
+            normed, w_ref[...], preferred_element_type=jnp.float32
+        ).astype(jnp.bfloat16)
+        low_ref[at, :] = lax.dot_general(
+            normed, down_ref[...], (((1,), (1,)), ((), ())), preferred_element_type=jnp.float32
+        ).astype(jnp.bfloat16)
+
     for k in range(n):
-        zc = jnp.where(2 * z < n, k, n - 1 - k)
+        zc = order(k)
         here = (zc == z) & (s == f)
         away = jnp.logical_not(here)
-        block = out_ref.at[piece(zc)]
+        block = seq_ref.at[piece(zc)]
         arrive = remote(block, block, send_sib.at[k], recv_a.at[zc], tp=1 - c)
         pl.when(away)(arrive.wait_recv)
         pl.when(here)(local.wait)
@@ -397,6 +465,9 @@
         sib = remote(block, block, send_sib.at[k], recv_b.at[zc], tp=1 - c)
         pl.when(away)(sib.start)
         pending.append((zc, away, sib, go_up, up, go_down, down))
+        if k > 0:
+            finish(k - 1)
+    finish(n - 1)
     pl.when(own)(local_r.wait)
     for k, copy in enumerate(sends):
         if k == 0:
@@ -408,26 +479,38 @@
     for zc, away, sib, go_up, up, go_down, down in pending:
         pl.when(go_up)(up.wait_send)
         pl.when(go_down)(down.wait_send)
-        other = out_ref.at[pl.ds(pl.multiple_of(zc * rows + (1 - c) * half, half), half)]
-        came = remote(other, other, send_sib.at[0], recv_b.at[zc], tp=1 - c)
-        pl.when(away)(came.wait_recv)
         pl.when(away)(sib.wait_send)
         came_r = remote(ret_ref, rout_ref.at[zc], send_r.at[0], recv_r.at[zc], tp=1 - c)
         pl.when(away)(came_r.wait_recv)
 
 
-def gather_positions(tokens, retain, n, fs_size, tp_size, hpd):
+def interleaved(weight):
+    width, hpd, columns = weight.shape
+    parts = columns // 128
+    return jnp.swapaxes(weight.reshape(width, hpd, parts, 128), 1, 2).reshape(-1, 128)
+
+
+def gather_positions(tokens, retain, gain, down, weights, n, fs_size, tp_size, hpd):
     rows, width = tokens.shape
     dma = pltpu.SemaphoreType.DMA
+    flat = [interleaved(weight) for weight in weights]
+    columns = sum(weight.shape[2] for weight in weights)
+    vmem = pl.BlockSpec(memory_space=pltpu.VMEM)
+    anywhere = pl.BlockSpec(memory_space=pl.ANY)
     return pl.pallas_call(
         functools.partial(gather_kernel, n, fs_size, tp_size, hpd),
         out_shape=(
-            jax.ShapeDtypeStruct((n * rows, width), tokens.dtype),
+            jax.ShapeDtypeStruct((n * rows, columns), jnp.bfloat16),
+            jax.ShapeDtypeStruct((n * rows, down.shape[0]), jnp.bfloat16),
             jax.ShapeDtypeStruct((n,) + retain.shape, retain.dtype),
         ),
-        in_specs=[pl.BlockSpec(memory_space=pltpu.VMEM)] * 2,
-        out_specs=(pl.BlockSpec(memory_space=pl.ANY), pl.BlockSpec(memory_space=pl.ANY)),
+        in_specs=[vmem] * 4 + [anywhere] * 6,
+        out_specs=(vmem, vmem, anywhere),
         scratch_shapes=[
+            pltpu.VMEM((n * rows, width), jnp.bfloat16),
+            pltpu.VMEM((5,) + flat[0].shape, jnp.bfloat16),
+            pltpu.VMEM(flat[5].shape, jnp.bfloat16),
+            pltpu.VMEM((width, columns), jnp.bfloat16),
             dma((n,)),
             dma((n,)),
             dma((n,)),
@@ -437,9 +520,137 @@
             dma((n,)),
             dma((hpd * fs_size,)),
             dma((2,)),
+            dma((6,)),
         ],
         compiler_params=pltpu.CompilerParams(collective_id=0, has_side_effects=True),
-    )(tokens, retain)
+    )(tokens, retain, gain, down, *flat)
+
+
+def mix_kernel(
+    hpd,
+    tp_size,
+    lam_ref,
+    proj_ref,
+    low_ref,
+    ret_ref,
+    up_ref,
+    bias_ref,
+    qg_ref,
+    kg_ref,
+    mg_ref,
+    sg_ref,
+    init_ref,
+    out_ref,
+):
+    z, f, c = lax.axis_index("sp"), lax.axis_index("fs"), lax.axis_index("tp")
+    slot = lax.rem(z, hpd)
+    seq = z // hpd
+    head = (f * tp_size + c) * hpd + slot
+    f32, bf16 = jnp.float32, jnp.bfloat16
+    length = proj_ref.shape[0]
+    lane = lax.broadcasted_iota(jnp.int32, (1, 2 * HD_A), 1)
+    first = lane < HD_A
+
+    def unit(cols, gain):
+        x = proj_ref[:, cols].astype(f32)
+        sq = x * x
+        m0 = jnp.sum(jnp.where(first, sq, 0.0), axis=-1, keepdims=True) / HD_A
+        m1 = jnp.sum(jnp.where(first, 0.0, sq), axis=-1, keepdims=True) / HD_A
+        r = jnp.where(first, lax.rsqrt(m0 + norm_eps), lax.rsqrt(m1 + norm_eps))
+        return (x * r * gain).astype(bf16)
+
+    q_gain = jnp.concatenate([qg_ref[...], qg_ref[...]], axis=1)
+    k_pair = kg_ref[pl.ds(head, 1)]
+    k_gain = jnp.concatenate([k_pair[:, 0], k_pair[:, 1]], axis=1)
+    q_unit = unit(slice(0, 128), q_gain)
+    k_unit = unit(slice(128, 256), k_gain)
+    zero = jnp.zeros_like(q_unit)
+    q_maps = (jnp.where(first, q_unit, zero), jnp.where(first, zero, q_unit))
+    tile = 2 * BLK
+    key_b = lax.broadcasted_iota(jnp.int32, (tile, tile), 1) // BLK
+    query_b = lax.broadcasted_iota(jnp.int32, (tile, tile), 0) // BLK
+    allowed = query_b >= key_b
+    lam = lam_ref[head]
+    for i in range(length // tile):
+        at = slice(i * tile, (i + 1) * tile)
+        parts = []
+        for m in range(2):
+            q = q_maps[m][at]
+            diag = (
+                lax.dot_general(
+                    q, k_unit[at], (((1,), (1,)), ((), ())), preferred_element_type=f32
+                )
+                * HD_A ** (-0.5)
+            )
+            diag = jnp.where(allowed, diag, -jnp.inf)
+            top = jnp.max(diag, axis=-1, keepdims=True)
+            if i > 0:
+                past = (
+                    lax.dot_general(
+                        q,
+                        k_unit[: i * tile],
+                        (((1,), (1,)), ((), ())),
+                        preferred_element_type=f32,
+                    )
+                    * HD_A ** (-0.5)
+                )
+                top = jnp.maximum(top, jnp.max(past, axis=-1, keepdims=True))
+            raised = jnp.exp(diag - top)
+            total = jnp.sum(raised, axis=-1, keepdims=True)
+            acc = jnp.dot(raised.astype(bf16), proj_ref[at, 256:384], preferred_element_type=f32)
+            if i > 0:
+                raised = jnp.exp(past - top)
+                total = total + jnp.sum(raised, axis=-1, keepdims=True)
+                acc = acc + jnp.dot(
+                    raised.astype(bf16), proj_ref[: i * tile, 256:384], preferred_element_type=f32
+                )
+            parts.append(acc / total)
+        diff = parts[0] - lam * parts[1]
+        scale = lax.rsqrt(jnp.mean(diff * diff, axis=-1, keepdims=True) + norm_eps)
+        out_ref[at, :DV_A] = (diff * scale * mg_ref[...]).astype(bf16)
+
+    up = up_ref[:, pl.ds(pl.multiple_of(head * HDK, HDK), HDK)]
+    bias = bias_ref[pl.ds(head, 1), :]
+    r64 = lax.broadcasted_iota(jnp.int32, (BLK, BLK), 0)
+    c64 = lax.broadcasted_iota(jnp.int32, (BLK, BLK), 1)
+    causal = r64 >= c64
+    lower = causal.astype(f32)
+    eye_k = lax.broadcasted_iota(jnp.int32, (HDK, HDK), 0) == lax.broadcasted_iota(
+        jnp.int32, (HDK, HDK), 1
+    )
+    pre = jnp.dot(low_ref[...], up, preferred_element_type=f32) + bias
+    log_sig = jnp.minimum(pre, 0.0) - jnp.log1p(jnp.exp(-jnp.abs(pre)))
+    log_sig = log_sig / decay_tau
+    state = init_ref[pl.ds(seq, 1), pl.ds(slot, 1)].reshape(HDK, HDV)
+    rows = ret_ref.shape[2]
+    per = rows // BLK
+    for b in range(length // BLK):
+        at = slice(b * BLK, (b + 1) * BLK)
+        ret = ret_ref[b // per, pl.ds(head, 1), :][:, (b % per) * BLK : (b % per + 1) * BLK]
+        column = jnp.sum(jnp.where(r64 == c64, ret, 0.0), axis=-1, keepdims=True)
+        logs = log_sig[at] + column
+        run = jnp.dot(
+            lower, logs, preferred_element_type=f32, precision=lax.Precision.HIGHEST
+        )
+        pivot = run[BLK // 2 : BLK // 2 + 1]
+        last = run[BLK - 1 : BLK]
+        q = proj_ref[at, 384:512].astype(f32) * HDK ** (-0.5)
+        k = proj_ref[at, 512:640].astype(f32)
+        v = proj_ref[at, 640:896]
+        qs = (q * jnp.exp(run - pivot)).astype(bf16)
+        ks = (k * jnp.exp(pivot - run)).astype(bf16)
+        inner = lax.dot_general(qs, ks, (((1,), (1,)), ((), ())), preferred_element_type=f32)
+        inner = jnp.where(causal, inner, 0.0).astype(bf16)
+        raw = jnp.dot(inner, v, preferred_element_type=f32) + jnp.dot(
+            (q * jnp.exp(run)).astype(bf16), state.astype(bf16), preferred_element_type=f32
+        )
+        faded = (k * jnp.exp(last - run)).astype(bf16)
+        keep = jnp.sum(jnp.where(eye_k, jnp.exp(last), 0.0), axis=-1, keepdims=True)
+        state = state * keep + lax.dot_general(
+            faded, v, (((0,), (0,)), ((), ())), preferred_element_type=f32
+        )
+        scale = lax.rsqrt(jnp.mean(raw * raw, axis=-1, keepdims=True) + norm_eps)
+        out_ref[at, DV_A:] = (raw * scale * sg_ref[...]).astype(bf16)
 
 
 def exchange_kernel(
@@ -572,65 +783,37 @@
 ):
     n, fs_size, tp_size = lax.axis_size("sp"), lax.axis_size("fs"), lax.axis_size("tp")
     hpd = query_attend.shape[1]
-    z = lax.axis_index("sp")
-    slot = lax.rem(z, hpd)
-    seq = z // hpd
-    head = (lax.axis_index("fs") * tp_size + lax.axis_index("tp")) * hpd + slot
-    rows = tokens.shape[1]
-    positions, retained = gather_positions(
-        tokens[0], jnp.transpose(log_retain[0]), n, fs_size, tp_size, hpd
-    )
-    retain = lax.dynamic_index_in_dim(retained, head, 1, False).reshape(n * rows)
-    normed = rms_scale(positions, norm_gain).astype(jnp.bfloat16)
-
-    def project(weight):
-        return jnp.dot(
-            normed,
-            lax.dynamic_index_in_dim(weight, slot, 1, False),
-            preferred_element_type=jnp.float32,
-        ).astype(jnp.bfloat16)
-
-    length = n * rows
-    q_unit = rms_scale(project(query_attend).reshape(length, 2, HD_A), query_gain)
-    k_unit = rms_scale(
-        project(key_attend).reshape(length, 2, HD_A), lax.dynamic_index_in_dim(key_gain, head, 0, False)
-    )
-    v_attend = project(value_attend)
-    scores = jnp.einsum(
-        "qmd,kmd->mqk",
-        q_unit.astype(jnp.bfloat16),
-        k_unit.astype(jnp.bfloat16),
-        preferred_element_type=jnp.float32,
-    ) * HD_A ** (-0.5)
-    blocks = jnp.arange(length, dtype=jnp.int32) // BLK
-    scores = jnp.where(blocks[:, None] >= blocks[None, :], scores, -jnp.inf)
-    raised = jnp.exp(scores - jnp.max(scores, axis=-1, keepdims=True))
-    totals = jnp.sum(raised, axis=-1, keepdims=True)
-    sums = jnp.einsum(
-        "mqk,kv->mqv", raised.astype(jnp.bfloat16), v_attend, preferred_element_type=jnp.float32
-    )
-    lam = lax.dynamic_index_in_dim(diff_lambda, head, 0, False)
-    diff_raw = sums[0] / totals[0] - lam * sums[1] / totals[1]
-    attend_out = rms_scale(diff_raw, mix_gain).astype(jnp.bfloat16)
-    low_rank = jnp.dot(normed, decay_down, preferred_element_type=jnp.float32).astype(jnp.bfloat16)
-    pre_act = jnp.dot(
+    weights = (query_attend, key_attend, value_attend, query_linear, key_linear, value_linear)
+    projected, low_rank, retained = gather_positions(
+        tokens[0],
+        jnp.transpose(log_retain[0]),
+        norm_gain[None],
+        jnp.transpose(decay_down),
+        weights,
+        n,
+        fs_size,
+        tp_size,
+        hpd,
+    )
+    vmem = pl.BlockSpec(memory_space=pltpu.VMEM)
+    mixed = pl.pallas_call(
+        functools.partial(mix_kernel, hpd, tp_size),
+        out_shape=jax.ShapeDtypeStruct((projected.shape[0], DV_A + HDV), jnp.bfloat16),
+        in_specs=[pl.BlockSpec(memory_space=pltpu.SMEM)] + [vmem] * 10,
+        out_specs=vmem,
+    )(
+        diff_lambda,
+        projected,
         low_rank,
-        lax.dynamic_index_in_dim(decay_up, head, 1, False),
-        preferred_element_type=jnp.float32,
-    ) + lax.dynamic_index_in_dim(decay_bias, head, 0, False)
-    log_decay = jax.nn.log_sigmoid(pre_act) / decay_tau + retain[:, None]
-    start = lax.dynamic_index_in_dim(
-        lax.dynamic_index_in_dim(init_state, seq, 0, False), slot, 0, False
-    )
-    _, _, inside, reaching = linear_blocks(
-        project(query_linear).astype(jnp.float32)[:, None] * HDK ** (-0.5),
-        project(key_linear).astype(jnp.float32)[:, None],
-        project(value_linear).astype(jnp.float32)[:, None],
-        log_decay[:, None],
-    )
-    linear_raw = inside[:, 0] + jnp.dot(reaching[:, 0], start, precision=lax.Precision.HIGHEST)
-    linear_out = rms_scale(linear_raw, state_gain).astype(jnp.bfloat16)
-    mixed = jnp.concatenate([attend_out, linear_out], axis=1)
+        retained,
+        decay_up.reshape(decay_up.shape[0], -1),
+        decay_bias,
+        query_gain[None],
+        key_gain,
+        mix_gain[None],
+        state_gain[None],
+        init_state,
+    )
     arrived = exchange_heads(mixed, n, fs_size, tp_size, hpd)
     heads = arrived.shape[0]
     out = jnp.einsum(

time: 138 us -> 88.9 us (0.64)
  matrix products: 35 us -> 5.16 us
  local copies, waits for them, and re-layouts: 21.8 us -> 3.07 us
  Pallas kernels: 65.5 us -> 80.3 us
  other arithmetic: 14 us -> 0 us
    dot_general x41 -> x0, matrix products: 29.8 us -> none  [the longest x8 6.71 us: advance(): jnp.einsum('jwo,wos->jws', question_patch_lines * jnp.exp(running_state),...]
    dynamic_slice x15 -> x0, local copies, waits for them, and re-layouts: 18.4 us -> none  [the longest x4 10.1 us: project(): lax.dynamic_index_in_dim(weight, slot, 1, False)]
    pallas_call x0 -> x1, Pallas kernels: none -> 7.55 us  [pair_body(): pl.pallas_call(functools.partial(mix_kernel, hpd, tp_size), out_shape=jax...]
    reduce_sum x3 -> x0, other arithmetic: 6.43 us -> none  [the longest x2 4.19 us: rms_scale(): jnp.mean(widened * widened, axis=-1, keepdims=True) + norm_eps]
    pallas_call x1, Pallas kernels: 40.8 us -> 47.1 us  [gather_positions(): pl.pallas_call(functools.partial(gather_kernel, n, fs_size, tp_size, hpd)...]
    dynamic_update_slice x8 -> x0, other arithmetic: 5.02 us -> none  [linear_blocks(): lax.scan(advance, start_carry, (split_blocks(queries), split_blocks(keys_...]
    unnamed x30 -> x5, local copies, waits for them, and re-layouts: 1.9 us -> 3.07 us
where the time goes in v2:
time: 88.9 us; the launch traced here: 88.6 us
  Pallas kernels  80.3 us (90%)
  matrix products  5.16 us (6%)
  local copies, waits for them, and re-layouts  3.07 us (3%)
    pallas_call x1, Pallas kernels, gather_positions(): pl.pallas_call(functools.partial(gather_kernel, n, fs_size, tp_size, hpd)...  47.1 us
    pallas_call x1, Pallas kernels, exchange_heads(): pl.pallas_call(functools.partial(exchange_kernel, n, fs_size, tp_size, hp...  25.6 us
    pallas_call x1, Pallas kernels, pair_body(): pl.pallas_call(functools.partial(mix_kernel, hpd, tp_size), out_shape=jax...  7.55 us
    dot_general x1, matrix products, pair_body(): jnp.einsum('htw,hwo->to', arrived[:, :, DV_A:], output_linear.reshape(hea...  3.69 us
    unnamed x5, local copies, waits for them, and re-layouts  3.07 us

profile of v2, /device:TPU:11, one launch (start us, length us, event | category | flops | bytes accessed | tf_op | source)
XLA Modules:
  0.0 88.6 jit_solution(15790482453717172241)
XLA Ops:
  0.0 0.0 copy-start
  0.0 1.6 %copy-done = bf16[1024,1024]{1,0:T(8,128)(2,1)S(1)} copy-done((bf16[1024,1024]{1,0:T(8,128)(2,1)S(1)}, bf16[1024,1024]{1,0:T(8,128)(2,1)}, u32[]{:S(2)}) %copy-start) | copy-done | bytes 2097176
  1.6 1.5 %copy.24 = bf16[4,8,8,128]{3,1,2,0:T(8,128)(2,1)} copy(bf16[4,8,8,128]{3,2,1,0:T(8,128)(2,1)} %bitcast.50) | data formatting | bytes 131072
  3.1 47.1 %shard_map.190 = (bf16[512,896]{1,0:T(8,128)(2,1)}, bf16[512,32]{1,0:T(8,128)(2,1)}, f32[4,8,128]{2,1,0:T(8,128)}) custom-call(bf16[128,2048]{1,0:T(8,128)(2,1)} %bitcast.47, f32[8,128]{1,0:T(8,128)} %bitcast.52, f32[1,2048]{1,0:T(1,128)} %bitcast.51, bf16[32,2048]{1,0:T(8,128)(2,1)} %bitcast.49, bf16[4096,128]{1,0:T(8,128)(2,1)} %bitcast.42, ...), custom_call_target="tpu_custom_call" | custom-call | tf_op jit(solution)/shard_map/pallas_call | solution.py:500
  50.2 7.5 %shard_map.191.mix_ref = bf16[512,384]{1,0:T(8,128)(2,1)} custom-call(f32[8]{0:T(128)} %lam_ref.1, bf16[512,896]{1,0:T(8,128)(2,1)} %get-tuple-element.8.proj_ref, bf16[512,32]{1,0:T(8,128)(2,1)} %get-tuple-element.9.low_ref, f32[4,8,128]{2,1,0:T(8,128)} %get-tuple-element.10.ret_ref, bf16[32,1024]{1,0:T(8,128)(2,1)} %bitcast.48, f32[8,128]{1,0:T(8,128)} %bias_ref.1, ...), custom_call_target="tpu_custom_call" | custom-call | tf_op jit(solution)/shard_map/pallas_call | solution.py:799
  57.8 25.6 %shard_map.192 = bf16[8,128,384]{2,1,0:T(8,128)(2,1)} custom-call(bf16[512,384]{1,0:T(8,128)(2,1)} %shard_map.191.mix_ref), custom_call_target="tpu_custom_call" | custom-call | tf_op jit(solution)/shard_map/pallas_call | solution.py:743
  83.4 0.0 copy-start.1
  83.4 1.5 %convolution_bitcast_fusion = f32[128,1024]{1,0:T(8,128)S(1)} fusion(bf16[8,128,1024]{2,1,0:T(8,128)(2,1)S(1)} %bitcast.39, bf16[8,128,384]{2,1,0:T(8,128)(2,1)} %shard_map.192), kind=kOutput, calls=%fused_computation | convolution fusion | flops 268435456 | bytes 2883584 | tf_op jit(solution)/shard_map/htw,hwo->to/dot_general | solution.py:819
  84.9 0.0 copy-done.1
  84.9 3.7 %fusion.2 = bf16[1,128,1024]{2,1,0:T(8,128)(2,1)} fusion(f32[128,1024]{1,0:T(8,128)S(1)} %convolution_bitcast_fusion, bf16[8,256,1024]{2,1,0:T(8,128)(2,1)} %bitcast.40, bf16[8,128,384]{2,1,0:T(8,128)(2,1)S(1)} %copy-done.1), kind=kOutput, calls=%fused_computation.4 | convolution fusion | flops 537133056 | bytes 5505024 | tf_op jit(solution)/shard_map/htw,hwo->to/dot_general | solution.py:824
Async XLA Ops:
  0.0 1.6 %copy-start = (bf16[1024,1024]{1,0:T(8,128)(2,1)S(1)}, bf16[1024,1024]{1,0:T(8,128)(2,1)}, u32[]{:S(2)}) copy-start(bf16[1024,1024]{1,0:T(8,128)(2,1)} %param.38) | copy-start | bytes 6291460
  83.4 1.5 %copy-start.1 = (bf16[8,128,384]{2,1,0:T(8,128)(2,1)S(1)}, bf16[8,128,384]{2,1,0:T(8,128)(2,1)}, u32[]{:S(2)}) copy-start(bf16[8,128,384]{2,1,0:T(8,128)(2,1)} %shard_map.192) | copy-start | bytes 2359300

commit v3 on v2

--- a/solution.py
+++ b/solution.py
@@ -330,13 +330,17 @@
     low_ref,
     rout_ref,
     seq_ref,
+    relay_ref,
     raw_ref,
     raw_v_ref,
     w_ref,
     recv_a,
     recv_b,
+    recv_l,
     recv_r,
-    send_a,
+    send_x,
+    send_row,
+    send_rl,
     send_up,
     send_down,
     send_sib,
@@ -347,6 +351,8 @@
     z, f, c = lax.axis_index("sp"), lax.axis_index("fs"), lax.axis_index("tp")
     rows, width = tok_ref.shape
     half = rows // tp_size
+    pieces = recv_l.shape[0]
+    prow = half // pieces
     loads = [
         pltpu.make_async_copy(ref, raw_ref.at[i], wsem.at[i])
         for i, ref in enumerate((wq_ref, wk_ref, wv_ref, lq_ref, lk_ref))
@@ -355,31 +361,17 @@
     for load in loads:
         load.start()
     group_barrier(n, fs_size, tp_size)
+    s = z // hpd
+    own = s == f
+    strange = jnp.logical_not(own)
+
+    def nearest(seq):
+        return jnp.minimum(jnp.maximum(z, seq * hpd), seq * hpd + hpd - 1)
+
+    def piece(zc, core, p):
+        return seq_ref.at[pl.ds(pl.multiple_of(zc * rows + core * half + p * prow, prow), prow)]
+
     lo = f * hpd
-    hi = lo + hpd - 1
-    near = jnp.minimum(jnp.maximum(z, lo), hi)
-    own = near == z
-
-    def piece(zc):
-        return pl.ds(pl.multiple_of(zc * rows + c * half, half), half)
-
-    mine = pl.ds(pl.multiple_of(c * half, half), half)
-    sends = []
-    for k in range(fs_size):
-        x = lax.rem(f + k, fs_size)
-        copy = remote(
-            tok_ref.at[mine], seq_ref.at[piece(z)], send_a.at[k], recv_a.at[z], sp=near, fs=x
-        )
-        if k == 0:
-            pl.when(jnp.logical_not(own))(copy.start)
-        else:
-            copy.start()
-        sends.append(copy)
-    full = pl.ds(pl.multiple_of(z * rows, rows), rows)
-    local = pltpu.make_async_copy(tok_ref, seq_ref.at[full], loc.at[0])
-    local_r = pltpu.make_async_copy(ret_ref, rout_ref.at[z], loc.at[1])
-    pl.when(own)(local.start)
-    pl.when(own)(local_r.start)
     rsends = []
     for j in range(hpd):
         for k in range(fs_size):
@@ -396,6 +388,22 @@
             go = jnp.logical_not((there == z) & (x == f))
             pl.when(go)(copy.start)
             rsends.append((go, copy))
+    sends = []
+    for p in range(pieces):
+        mine = tok_ref.at[pl.ds(pl.multiple_of(c * half + p * prow, prow), prow)]
+        there = relay_ref.at[pl.ds(p * prow, prow)]
+        over = remote(mine, piece(z, c, p), send_x.at[p], recv_a.at[z, p], fs=1 - f)
+        pl.when(own)(over.start)
+        lent = remote(mine, there, send_x.at[p], recv_l.at[p], fs=1 - f)
+        pl.when(strange)(lent.start)
+        along = remote(mine, piece(z, c, p), send_row.at[p], recv_a.at[z, p], sp=nearest(f))
+        pl.when(strange)(along.start)
+        sends += [(own, over), (strange, lent), (strange, along)]
+    full = pl.ds(pl.multiple_of(z * rows, rows), rows)
+    local = pltpu.make_async_copy(tok_ref, seq_ref.at[full], loc.at[0])
+    local_r = pltpu.make_async_copy(ret_ref, rout_ref.at[z], loc.at[1])
+    pl.when(own)(local.start)
+    pl.when(own)(local_r.start)
 
     slot = lax.rem(z, hpd)
     step = 128
@@ -416,70 +424,81 @@
 
         lax.fori_loop(0, width // step, one, 0)
 
-    for i in range(5):
-        loads[i].wait()
-        pick(raw_ref.at[i], slice(i * 128, (i + 1) * 128), 1, 0)
-    loads[5].wait()
-    for part in range(2):
-        pick(raw_v_ref, slice((5 + part) * 128, (6 + part) * 128), 2, part)
-
-    s = z // hpd
+    def pick_all(first, last):
+        for i in range(first, min(last, 5)):
+            loads[i].wait()
+            pick(raw_ref.at[i], slice(i * 128, (i + 1) * 128), 1, 0)
+        if last > 5:
+            loads[5].wait()
+            for part in range(2):
+                pick(raw_v_ref, slice((5 + part) * 128, (6 + part) * 128), 2, part)
+
     mlo = s * hpd
     mhi = mlo + hpd - 1
-    pending = []
-
-    def order(k):
-        return jnp.where(2 * z < n, k, n - 1 - k)
-
-    def finish(k):
-        zc = order(k)
-        away = jnp.logical_not((zc == z) & (s == f))
-        other = seq_ref.at[pl.ds(pl.multiple_of(zc * rows + (1 - c) * half, half), half)]
-        came = remote(other, other, send_sib.at[0], recv_b.at[zc], tp=1 - c)
-        pl.when(away)(came.wait_recv)
-        at = pl.ds(pl.multiple_of(zc * rows, rows), rows)
-        x = seq_ref[at, :].astype(jnp.float32)
+
+    def pass_on(p):
+        held = relay_ref.at[pl.ds(p * prow, prow)]
+        lent = remote(held, piece(z, c, p), send_rl.at[p], recv_l.at[p], sp=nearest(1 - f))
+        pl.when(own)(lent.wait_recv)
+        along = remote(held, piece(z, c, p), send_rl.at[p], recv_a.at[z, p], sp=nearest(1 - f))
+        pl.when(own)(along.start)
+        sends.append((own, along))
+        for k in range(n):
+            zc = jnp.where(2 * z < n, n - 1 - k, k)
+            away = jnp.logical_not((zc == z) & own)
+            block = piece(zc, c, p)
+            arrive = remote(block, block, send_sib.at[k, p], recv_a.at[zc, p], tp=1 - c)
+            pl.when(away)(arrive.wait_recv)
+            up = remote(
+                block, block, send_up.at[k, p], recv_a.at[zc, p], sp=jnp.minimum(z + 1, n - 1)
+            )
+            go_up = (zc <= z) & (z + 1 <= mhi)
+            pl.when(go_up)(up.start)
+            down = remote(
+                block, block, send_down.at[k, p], recv_a.at[zc, p], sp=jnp.maximum(z - 1, 0)
+            )
+            go_down = (zc >= z) & (z - 1 >= mlo)
+            pl.when(go_down)(down.start)
+            sib = remote(block, block, send_sib.at[k, p], recv_b.at[zc, p], tp=1 - c)
+            pl.when(away)(sib.start)
+            sends.extend([(go_up, up), (go_down, down), (away, sib)])
+
+    def finish(p):
+        for zc in range(n):
+            away = jnp.logical_not((zc == z) & own)
+            other = piece(zc, 1 - c, p)
+            came = remote(other, other, send_sib.at[zc, p], recv_b.at[zc, p], tp=1 - c)
+            pl.when(away)(came.wait_recv)
+        spots = [
+            slice(zc * rows + core * half + p * prow, zc * rows + core * half + (p + 1) * prow)
+            for zc in range(n)
+            for core in range(tp_size)
+        ]
+        x = jnp.concatenate([seq_ref[spot, :] for spot in spots], axis=0).astype(jnp.float32)
         scale = lax.rsqrt(jnp.mean(x * x, axis=-1, keepdims=True) + norm_eps)
         normed = (x * scale * gain_ref[...]).astype(jnp.bfloat16)
-        proj_ref[at, :] = jnp.dot(
-            normed, w_ref[...], preferred_element_type=jnp.float32
-        ).astype(jnp.bfloat16)
-        low_ref[at, :] = lax.dot_general(
+        made = jnp.dot(normed, w_ref[...], preferred_element_type=jnp.float32).astype(jnp.bfloat16)
+        low = lax.dot_general(
             normed, down_ref[...], (((1,), (1,)), ((), ())), preferred_element_type=jnp.float32
         ).astype(jnp.bfloat16)
-
-    for k in range(n):
-        zc = order(k)
-        here = (zc == z) & (s == f)
-        away = jnp.logical_not(here)
-        block = seq_ref.at[piece(zc)]
-        arrive = remote(block, block, send_sib.at[k], recv_a.at[zc], tp=1 - c)
-        pl.when(away)(arrive.wait_recv)
-        pl.when(here)(local.wait)
-        up = remote(block, block, send_up.at[k], recv_a.at[zc], sp=jnp.minimum(z + 1, n - 1))
-        go_up = (zc <= z) & (z + 1 <= mhi)
-        pl.when(go_up)(up.start)
-        down = remote(block, block, send_down.at[k], recv_a.at[zc], sp=jnp.maximum(z - 1, 0))
-        go_down = (zc >= z) & (z - 1 >= mlo)
-        pl.when(go_down)(down.start)
-        sib = remote(block, block, send_sib.at[k], recv_b.at[zc], tp=1 - c)
-        pl.when(away)(sib.start)
-        pending.append((zc, away, sib, go_up, up, go_down, down))
-        if k > 0:
-            finish(k - 1)
-    finish(n - 1)
+        for i, spot in enumerate(spots):
+            proj_ref[spot, :] = made[i * prow : (i + 1) * prow]
+            low_ref[spot, :] = low[i * prow : (i + 1) * prow]
+
+    pl.when(own)(local.wait)
+    pass_on(0)
+    pick_all(0, 3)
+    for p in range(1, pieces):
+        pass_on(p)
+        if p == 1:
+            pick_all(3, 6)
+        finish(p - 1)
+    finish(pieces - 1)
     pl.when(own)(local_r.wait)
-    for k, copy in enumerate(sends):
-        if k == 0:
-            pl.when(jnp.logical_not(own))(copy.wait_send)
-        else:
-            copy.wait_send()
-    for go, copy in rsends:
+    for go, copy in rsends + sends:
         pl.when(go)(copy.wait_send)
-    for zc, away, sib, go_up, up, go_down, down in pending:
-        pl.when(go_up)(up.wait_send)
-        pl.when(go_down)(down.wait_send)
-        pl.when(away)(sib.wait_send)
+    for zc in range(n):
+        away = jnp.logical_not((zc == z) & own)
         came_r = remote(ret_ref, rout_ref.at[zc], send_r.at[0], recv_r.at[zc], tp=1 - c)
         pl.when(away)(came_r.wait_recv)
 
@@ -494,6 +513,7 @@
     rows, width = tokens.shape
     dma = pltpu.SemaphoreType.DMA
     flat = [interleaved(weight) for weight in weights]
+    pieces = max(1, rows // tp_size // 16)
     columns = sum(weight.shape[2] for weight in weights)
     vmem = pl.BlockSpec(memory_space=pltpu.VMEM)
     anywhere = pl.BlockSpec(memory_space=pl.ANY)
@@ -508,16 +528,20 @@
         out_specs=(vmem, vmem, anywhere),
         scratch_shapes=[
             pltpu.VMEM((n * rows, width), jnp.bfloat16),
+            pltpu.VMEM((rows // tp_size, width), jnp.bfloat16),
             pltpu.VMEM((5,) + flat[0].shape, jnp.bfloat16),
             pltpu.VMEM(flat[5].shape, jnp.bfloat16),
             pltpu.VMEM((width, columns), jnp.bfloat16),
+            dma((n, pieces)),
+            dma((n, pieces)),
+            dma((pieces,)),
             dma((n,)),
-            dma((n,)),
-            dma((n,)),
-            dma((fs_size,)),
-            dma((n,)),
-            dma((n,)),
-            dma((n,)),
+            dma((pieces,)),
+            dma((pieces,)),
+            dma((pieces,)),
+            dma((n, pieces)),
+            dma((n, pieces)),
+            dma((n, pieces)),
             dma((hpd * fs_size,)),
             dma((2,)),
             dma((6,)),
@@ -856,5 +880,5 @@
     out_specs = P(("grp", "fs"), "sp", "tp")
     fs_size, tp_size, sp_size = mesh.shape["fs"], mesh.shape["tp"], mesh.shape["sp"]
     pairs = MIXER_HEADS // tp_size
-    chosen = pair_body if pairs == sp_size and tp_size == 2 else body
+    chosen = pair_body if pairs == sp_size and tp_size == 2 and fs_size == 2 else body
     return jax.shard_map(chosen, mesh=mesh, in_specs=in_specs, out_specs=out_specs, check_vma=False)

time: 88.9 us -> 110 us (1.24)
  Pallas kernels: 80.3 us -> 102 us
    pallas_call x1, Pallas kernels: 47.1 us -> 73.9 us  [gather_positions(): pl.pallas_call(functools.partial(gather_kernel, n, fs_size, tp_size, hpd)...]
    pallas_call x1, Pallas kernels: 25.6 us -> 20.3 us  [exchange_heads(): pl.pallas_call(functools.partial(exchange_kernel, n, fs_size, tp_size, hp...]
where the time goes in v3:
time: 110 us
  Pallas kernels  102 us (93%)
  matrix products  5.15 us (5%)
  local copies, waits for them, and re-layouts  3.07 us (3%)
    pallas_call x1, Pallas kernels, gather_positions(): pl.pallas_call(functools.partial(gather_kernel, n, fs_size, tp_size, hpd)...  73.9 us
    pallas_call x1, Pallas kernels, exchange_heads(): pl.pallas_call(functools.partial(exchange_kernel, n, fs_size, tp_size, hp...  20.3 us
    pallas_call x1, Pallas kernels, pair_body(): pl.pallas_call(functools.partial(mix_kernel, hpd, tp_size), out_shape=jax...  7.55 us
    dot_general x1, matrix products, pair_body(): jnp.einsum('htw,hwo->to', arrived[:, :, DV_A:], output_linear.reshape(hea...  3.68 us
    unnamed x5, local copies, waits for them, and re-layouts  3.07 us

profile of v3, /device:TPU:11, one launch (start us, length us, event | category | flops | bytes accessed | tf_op | source)
XLA Modules:
  0.0 110.1 jit_solution(17075964299199661358)
XLA Ops:
  0.0 0.0 copy-start
  0.0 1.6 %copy-done = bf16[1024,1024]{1,0:T(8,128)(2,1)S(1)} copy-done((bf16[1024,1024]{1,0:T(8,128)(2,1)S(1)}, bf16[1024,1024]{1,0:T(8,128)(2,1)}, u32[]{:S(2)}) %copy-start) | copy-done | bytes 2097176
  1.6 1.5 %copy.24 = bf16[4,8,8,128]{3,1,2,0:T(8,128)(2,1)} copy(bf16[4,8,8,128]{3,2,1,0:T(8,128)(2,1)} %bitcast.50) | data formatting | bytes 131072
  3.1 73.9 %shard_map.190 = (bf16[512,896]{1,0:T(8,128)(2,1)}, bf16[512,32]{1,0:T(8,128)(2,1)}, f32[4,8,128]{2,1,0:T(8,128)}) custom-call(bf16[128,2048]{1,0:T(8,128)(2,1)} %bitcast.47, f32[8,128]{1,0:T(8,128)} %bitcast.52, f32[1,2048]{1,0:T(1,128)} %bitcast.51, bf16[32,2048]{1,0:T(8,128)(2,1)} %bitcast.49, bf16[4096,128]{1,0:T(8,128)(2,1)} %bitcast.42, ...), custom_call_target="tpu_custom_call" | custom-call | tf_op jit(solution)/shard_map/pallas_call | solution.py:520
  77.0 7.6 %shard_map.191.mix_ref = bf16[512,384]{1,0:T(8,128)(2,1)} custom-call(f32[8]{0:T(128)} %lam_ref.1, bf16[512,896]{1,0:T(8,128)(2,1)} %get-tuple-element.8.proj_ref, bf16[512,32]{1,0:T(8,128)(2,1)} %get-tuple-element.9.low_ref, f32[4,8,128]{2,1,0:T(8,128)} %get-tuple-element.10.ret_ref, bf16[32,1024]{1,0:T(8,128)(2,1)} %bitcast.48, f32[8,128]{1,0:T(8,128)} %bias_ref.1, ...), custom_call_target="tpu_custom_call" | custom-call | tf_op jit(solution)/shard_map/pallas_call | solution.py:823
  84.5 20.3 %shard_map.192 = bf16[8,128,384]{2,1,0:T(8,128)(2,1)} custom-call(bf16[512,384]{1,0:T(8,128)(2,1)} %shard_map.191.mix_ref), custom_call_target="tpu_custom_call" | custom-call | tf_op jit(solution)/shard_map/pallas_call | solution.py:767
  104.9 0.0 copy-start.1
  104.9 1.5 %convolution_bitcast_fusion = f32[128,1024]{1,0:T(8,128)S(1)} fusion(bf16[8,128,1024]{2,1,0:T(8,128)(2,1)S(1)} %bitcast.39, bf16[8,128,384]{2,1,0:T(8,128)(2,1)} %shard_map.192), kind=kOutput, calls=%fused_computation | convolution fusion | flops 268435456 | bytes 2883584 | tf_op jit(solution)/shard_map/htw,hwo->to/dot_general | solution.py:843
  106.4 0.0 copy-done.1
  106.4 3.7 %fusion.2 = bf16[1,128,1024]{2,1,0:T(8,128)(2,1)} fusion(f32[128,1024]{1,0:T(8,128)S(1)} %convolution_bitcast_fusion, bf16[8,256,1024]{2,1,0:T(8,128)(2,1)} %bitcast.40, bf16[8,128,384]{2,1,0:T(8,128)(2,1)S(1)} %copy-done.1), kind=kOutput, calls=%fused_computation.4 | convolution fusion | flops 537133056 | bytes 5505024 | tf_op jit(solution)/shard_map/htw,hwo->to/dot_general | solution.py:848
Async XLA Ops:
  0.0 1.6 %copy-start = (bf16[1024,1024]{1,0:T(8,128)(2,1)S(1)}, bf16[1024,1024]{1,0:T(8,128)(2,1)}, u32[]{:S(2)}) copy-start(bf16[1024,1024]{1,0:T(8,128)(2,1)} %param.38) | copy-start | bytes 6291460
  104.9 1.5 %copy-start.1 = (bf16[8,128,384]{2,1,0:T(8,128)(2,1)S(1)}, bf16[8,128,384]{2,1,0:T(8,128)(2,1)}, u32[]{:S(2)}) copy-start(bf16[8,128,384]{2,1,0:T(8,128)(2,1)} %shard_map.192) | copy-start | bytes 2359300

commit v4 on v3

--- a/solution.py
+++ b/solution.py
@@ -436,32 +436,40 @@
     mlo = s * hpd
     mhi = mlo + hpd - 1
 
-    def pass_on(p):
+    def relay(p):
         held = relay_ref.at[pl.ds(p * prow, prow)]
         lent = remote(held, piece(z, c, p), send_rl.at[p], recv_l.at[p], sp=nearest(1 - f))
         pl.when(own)(lent.wait_recv)
         along = remote(held, piece(z, c, p), send_rl.at[p], recv_a.at[z, p], sp=nearest(1 - f))
         pl.when(own)(along.start)
         sends.append((own, along))
+
+    def handle(zc, p, act, away):
+        block = piece(zc, c, p)
+        arrive = remote(block, block, send_sib.at[zc, p], recv_a.at[zc, p], tp=1 - c)
+        pl.when(away)(arrive.wait_recv)
+        up = remote(
+            block, block, send_up.at[zc, p], recv_a.at[zc, p], sp=jnp.minimum(z + 1, n - 1)
+        )
+        go_up = act & (zc <= z) & (z + 1 <= mhi)
+        pl.when(go_up)(up.start)
+        down = remote(
+            block, block, send_down.at[zc, p], recv_a.at[zc, p], sp=jnp.maximum(z - 1, 0)
+        )
+        go_down = act & (zc >= z) & (z - 1 >= mlo)
+        pl.when(go_down)(down.start)
+        sib = remote(block, block, send_sib.at[zc, p], recv_b.at[zc, p], tp=1 - c)
+        pl.when(away)(sib.start)
+        sends.extend([(go_up, up), (go_down, down), (away, sib)])
+
+    def early(p):
+        relay(p)
+        handle(z, p, z >= 0, strange)
+
+    def rest(p):
         for k in range(n):
             zc = jnp.where(2 * z < n, n - 1 - k, k)
-            away = jnp.logical_not((zc == z) & own)
-            block = piece(zc, c, p)
-            arrive = remote(block, block, send_sib.at[k, p], recv_a.at[zc, p], tp=1 - c)
-            pl.when(away)(arrive.wait_recv)
-            up = remote(
-                block, block, send_up.at[k, p], recv_a.at[zc, p], sp=jnp.minimum(z + 1, n - 1)
-            )
-            go_up = (zc <= z) & (z + 1 <= mhi)
-            pl.when(go_up)(up.start)
-            down = remote(
-                block, block, send_down.at[k, p], recv_a.at[zc, p], sp=jnp.maximum(z - 1, 0)
-            )
-            go_down = (zc >= z) & (z - 1 >= mlo)
-            pl.when(go_down)(down.start)
-            sib = remote(block, block, send_sib.at[k, p], recv_b.at[zc, p], tp=1 - c)
-            pl.when(away)(sib.start)
-            sends.extend([(go_up, up), (go_down, down), (away, sib)])
+            handle(zc, p, zc != z, zc != z)
 
     def finish(p):
         for zc in range(n):
@@ -486,13 +494,17 @@
             low_ref[spot, :] = low[i * prow : (i + 1) * prow]
 
     pl.when(own)(local.wait)
-    pass_on(0)
-    pick_all(0, 3)
-    for p in range(1, pieces):
-        pass_on(p)
-        if p == 1:
+    early(0)
+    for p in range(pieces):
+        if p + 1 < pieces:
+            early(p + 1)
+        rest(p)
+        if p == 0:
+            pick_all(0, 3)
+        if p == min(1, pieces - 1):
             pick_all(3, 6)
-        finish(p - 1)
+        if p > 0:
+            finish(p - 1)
     finish(pieces - 1)
     pl.when(own)(local_r.wait)
     for go, copy in rsends + sends:

time: 110 us -> 86.7 us (0.79)
  Pallas kernels: 102 us -> 78.1 us
    pallas_call x1, Pallas kernels: 73.9 us -> 46 us  [gather_positions(): pl.pallas_call(functools.partial(gather_kernel, n, fs_size, tp_size, hpd)...]
    pallas_call x1, Pallas kernels: 20.3 us -> 24.5 us  [exchange_heads(): pl.pallas_call(functools.partial(exchange_kernel, n, fs_size, tp_size, hp...]
where the time goes in v4:
time: 86.7 us; the launch traced here: 86.4 us
  Pallas kernels  78.1 us (90%)
  matrix products  5.15 us (6%)
  local copies, waits for them, and re-layouts  3.07 us (4%)
    pallas_call x1, Pallas kernels, gather_positions(): pl.pallas_call(functools.partial(gather_kernel, n, fs_size, tp_size, hpd)...  46 us
    pallas_call x1, Pallas kernels, exchange_heads(): pl.pallas_call(functools.partial(exchange_kernel, n, fs_size, tp_size, hp...  24.5 us
    pallas_call x1, Pallas kernels, pair_body(): pl.pallas_call(functools.partial(mix_kernel, hpd, tp_size), out_shape=jax...  7.56 us
    dot_general x1, matrix products, pair_body(): jnp.einsum('htw,hwo->to', arrived[:, :, DV_A:], output_linear.reshape(hea...  3.69 us
    unnamed x5, local copies, waits for them, and re-layouts  3.07 us

profile of v4, /device:TPU:11, one launch (start us, length us, event | category | flops | bytes accessed | tf_op | source)
XLA Modules:
  0.0 86.4 jit_solution(4446004331434372261)
XLA Ops:
  0.0 0.0 copy-start
  0.0 1.6 %copy-done = bf16[1024,1024]{1,0:T(8,128)(2,1)S(1)} copy-done((bf16[1024,1024]{1,0:T(8,128)(2,1)S(1)}, bf16[1024,1024]{1,0:T(8,128)(2,1)}, u32[]{:S(2)}) %copy-start) | copy-done | bytes 2097176
  1.6 1.5 %copy.24 = bf16[4,8,8,128]{3,1,2,0:T(8,128)(2,1)} copy(bf16[4,8,8,128]{3,2,1,0:T(8,128)(2,1)} %bitcast.50) | data formatting | bytes 131072
  3.1 46.0 %shard_map.190 = (bf16[512,896]{1,0:T(8,128)(2,1)}, bf16[512,32]{1,0:T(8,128)(2,1)}, f32[4,8,128]{2,1,0:T(8,128)}) custom-call(bf16[128,2048]{1,0:T(8,128)(2,1)} %bitcast.47, f32[8,128]{1,0:T(8,128)} %bitcast.52, f32[1,2048]{1,0:T(1,128)} %bitcast.51, bf16[32,2048]{1,0:T(8,128)(2,1)} %bitcast.49, bf16[4096,128]{1,0:T(8,128)(2,1)} %bitcast.42, ...), custom_call_target="tpu_custom_call" | custom-call | tf_op jit(solution)/shard_map/pallas_call | solution.py:532
  49.1 7.6 %shard_map.191.mix_ref = bf16[512,384]{1,0:T(8,128)(2,1)} custom-call(f32[8]{0:T(128)} %lam_ref.1, bf16[512,896]{1,0:T(8,128)(2,1)} %get-tuple-element.8.proj_ref, bf16[512,32]{1,0:T(8,128)(2,1)} %get-tuple-element.9.low_ref, f32[4,8,128]{2,1,0:T(8,128)} %get-tuple-element.10.ret_ref, bf16[32,1024]{1,0:T(8,128)(2,1)} %bitcast.48, f32[8,128]{1,0:T(8,128)} %bias_ref.1, ...), custom_call_target="tpu_custom_call" | custom-call | tf_op jit(solution)/shard_map/pallas_call | solution.py:835
  56.6 24.5 %shard_map.192 = bf16[8,128,384]{2,1,0:T(8,128)(2,1)} custom-call(bf16[512,384]{1,0:T(8,128)(2,1)} %shard_map.191.mix_ref), custom_call_target="tpu_custom_call" | custom-call | tf_op jit(solution)/shard_map/pallas_call | solution.py:779
  81.2 0.0 copy-start.1
  81.2 1.5 %convolution_bitcast_fusion = f32[128,1024]{1,0:T(8,128)S(1)} fusion(bf16[8,128,1024]{2,1,0:T(8,128)(2,1)S(1)} %bitcast.39, bf16[8,128,384]{2,1,0:T(8,128)(2,1)} %shard_map.192), kind=kOutput, calls=%fused_computation | convolution fusion | flops 268435456 | bytes 2883584 | tf_op jit(solution)/shard_map/htw,hwo->to/dot_general | solution.py:855
  82.7 0.0 copy-done.1
  82.7 3.7 %fusion.2 = bf16[1,128,1024]{2,1,0:T(8,128)(2,1)} fusion(f32[128,1024]{1,0:T(8,128)S(1)} %convolution_bitcast_fusion, bf16[8,256,1024]{2,1,0:T(8,128)(2,1)} %bitcast.40, bf16[8,128,384]{2,1,0:T(8,128)(2,1)S(1)} %copy-done.1), kind=kOutput, calls=%fused_computation.4 | convolution fusion | flops 537133056 | bytes 5505024 | tf_op jit(solution)/shard_map/htw,hwo->to/dot_general | solution.py:860
Async XLA Ops:
  0.0 1.6 %copy-start = (bf16[1024,1024]{1,0:T(8,128)(2,1)S(1)}, bf16[1024,1024]{1,0:T(8,128)(2,1)}, u32[]{:S(2)}) copy-start(bf16[1024,1024]{1,0:T(8,128)(2,1)} %param.38) | copy-start | bytes 6291460
  81.2 1.5 %copy-start.1 = (bf16[8,128,384]{2,1,0:T(8,128)(2,1)S(1)}, bf16[8,128,384]{2,1,0:T(8,128)(2,1)}, u32[]{:S(2)}) copy-start(bf16[8,128,384]{2,1,0:T(8,128)(2,1)} %shard_map.192) | copy-start | bytes 2359300

commit v5 on v4

--- a/solution.py
+++ b/solution.py
@@ -408,30 +408,29 @@
     slot = lax.rem(z, hpd)
     step = 128
 
-    def pick(source, target_cols, parts, part):
+    def pick(sources, target_cols, parts, part):
         span = step * parts * hpd
         sel = (
             lax.broadcasted_iota(jnp.int32, (step, span), 1)
             == (lax.broadcasted_iota(jnp.int32, (step, span), 0) * parts + part) * hpd + slot
         ).astype(jnp.bfloat16)
-
-        def one(i, carry):
-            block = source[pl.ds(pl.multiple_of(i * span, span), span), :]
-            w_ref[pl.ds(pl.multiple_of(i * step, step), step), target_cols] = jnp.dot(
+        for i in range(width // step):
+            blocks = [source[i * span : (i + 1) * span, :] for source in sources]
+            block = blocks[0] if len(blocks) == 1 else jnp.concatenate(blocks, axis=1)
+            w_ref[i * step : (i + 1) * step, target_cols] = jnp.dot(
                 sel, block, preferred_element_type=jnp.float32
             ).astype(jnp.bfloat16)
-            return carry
-
-        lax.fori_loop(0, width // step, one, 0)
 
     def pick_all(first, last):
-        for i in range(first, min(last, 5)):
-            loads[i].wait()
-            pick(raw_ref.at[i], slice(i * 128, (i + 1) * 128), 1, 0)
+        for i in range(first, min(last, 5), 2):
+            group = range(i, min(i + 2, 5))
+            for j in group:
+                loads[j].wait()
+            pick([raw_ref.at[j] for j in group], slice(i * 128, (group[-1] + 1) * 128), 1, 0)
         if last > 5:
             loads[5].wait()
             for part in range(2):
-                pick(raw_v_ref, slice((5 + part) * 128, (6 + part) * 128), 2, part)
+                pick([raw_v_ref], slice((5 + part) * 128, (6 + part) * 128), 2, part)
 
     mlo = s * hpd
     mhi = mlo + hpd - 1
@@ -500,9 +499,9 @@
             early(p + 1)
         rest(p)
         if p == 0:
-            pick_all(0, 3)
+            pick_all(0, 4)
         if p == min(1, pieces - 1):
-            pick_all(3, 6)
+            pick_all(4, 6)
         if p > 0:
             finish(p - 1)
     finish(pieces - 1)

time: 86.7 us -> 73.7 us (0.85)
  Pallas kernels: 78.1 us -> 65.1 us
    pallas_call x1, Pallas kernels: 46 us -> 33 us  [gather_positions(): pl.pallas_call(functools.partial(gather_kernel, n, fs_size, tp_size, hpd)...]
where the time goes in v5:
time: 73.7 us; the launch traced here: 73.4 us
  Pallas kernels  65.1 us (88%)
  matrix products  5.16 us (7%)
  local copies, waits for them, and re-layouts  3.07 us (4%)
    pallas_call x1, Pallas kernels, gather_positions(): pl.pallas_call(functools.partial(gather_kernel, n, fs_size, tp_size, hpd)...  33 us
    pallas_call x1, Pallas kernels, exchange_heads(): pl.pallas_call(functools.partial(exchange_kernel, n, fs_size, tp_size, hp...  24.5 us
    pallas_call x1, Pallas kernels, pair_body(): pl.pallas_call(functools.partial(mix_kernel, hpd, tp_size), out_shape=jax...  7.56 us
    dot_general x1, matrix products, pair_body(): jnp.einsum('htw,hwo->to', arrived[:, :, DV_A:], output_linear.reshape(hea...  3.69 us
    unnamed x5, local copies, waits for them, and re-layouts  3.07 us

profile of v5, /device:TPU:11, one launch (start us, length us, event | category | flops | bytes accessed | tf_op | source)
XLA Modules:
  0.0 73.4 jit_solution(9247181301118803354)
XLA Ops:
  0.0 0.0 copy-start
  0.0 1.6 %copy-done = bf16[1024,1024]{1,0:T(8,128)(2,1)S(1)} copy-done((bf16[1024,1024]{1,0:T(8,128)(2,1)S(1)}, bf16[1024,1024]{1,0:T(8,128)(2,1)}, u32[]{:S(2)}) %copy-start) | copy-done | bytes 2097176
  1.6 1.5 %copy.24 = bf16[4,8,8,128]{3,1,2,0:T(8,128)(2,1)} copy(bf16[4,8,8,128]{3,2,1,0:T(8,128)(2,1)} %bitcast.50) | data formatting | bytes 131072
  3.1 33.0 %shard_map.190 = (bf16[512,896]{1,0:T(8,128)(2,1)}, bf16[512,32]{1,0:T(8,128)(2,1)}, f32[4,8,128]{2,1,0:T(8,128)}) custom-call(bf16[128,2048]{1,0:T(8,128)(2,1)} %bitcast.47, f32[8,128]{1,0:T(8,128)} %bitcast.52, f32[1,2048]{1,0:T(1,128)} %bitcast.51, bf16[32,2048]{1,0:T(8,128)(2,1)} %bitcast.49, bf16[4096,128]{1,0:T(8,128)(2,1)} %bitcast.42, ...), custom_call_target="tpu_custom_call" | custom-call | tf_op jit(solution)/shard_map/pallas_call | solution.py:531
  36.1 7.6 %shard_map.191.mix_ref = bf16[512,384]{1,0:T(8,128)(2,1)} custom-call(f32[8]{0:T(128)} %lam_ref.1, bf16[512,896]{1,0:T(8,128)(2,1)} %get-tuple-element.8.proj_ref, bf16[512,32]{1,0:T(8,128)(2,1)} %get-tuple-element.9.low_ref, f32[4,8,128]{2,1,0:T(8,128)} %get-tuple-element.10.ret_ref, bf16[32,1024]{1,0:T(8,128)(2,1)} %bitcast.48, f32[8,128]{1,0:T(8,128)} %bias_ref.1, ...), custom_call_target="tpu_custom_call" | custom-call | tf_op jit(solution)/shard_map/pallas_call | solution.py:834
  43.6 24.5 %shard_map.192 = bf16[8,128,384]{2,1,0:T(8,128)(2,1)} custom-call(bf16[512,384]{1,0:T(8,128)(2,1)} %shard_map.191.mix_ref), custom_call_target="tpu_custom_call" | custom-call | tf_op jit(solution)/shard_map/pallas_call | solution.py:778
  68.2 0.0 copy-start.1
  68.2 1.5 %convolution_bitcast_fusion = f32[128,1024]{1,0:T(8,128)S(1)} fusion(bf16[8,128,1024]{2,1,0:T(8,128)(2,1)S(1)} %bitcast.39, bf16[8,128,384]{2,1,0:T(8,128)(2,1)} %shard_map.192), kind=kOutput, calls=%fused_computation | convolution fusion | flops 268435456 | bytes 2883584 | tf_op jit(solution)/shard_map/htw,hwo->to/dot_general | solution.py:854
  69.7 0.0 copy-done.1
  69.7 3.7 %fusion.2 = bf16[1,128,1024]{2,1,0:T(8,128)(2,1)} fusion(f32[128,1024]{1,0:T(8,128)S(1)} %convolution_bitcast_fusion, bf16[8,256,1024]{2,1,0:T(8,128)(2,1)} %bitcast.40, bf16[8,128,384]{2,1,0:T(8,128)(2,1)S(1)} %copy-done.1), kind=kOutput, calls=%fused_computation.4 | convolution fusion | flops 537133056 | bytes 5505024 | tf_op jit(solution)/shard_map/htw,hwo->to/dot_general | solution.py:859
Async XLA Ops:
  0.0 1.6 %copy-start = (bf16[1024,1024]{1,0:T(8,128)(2,1)S(1)}, bf16[1024,1024]{1,0:T(8,128)(2,1)}, u32[]{:S(2)}) copy-start(bf16[1024,1024]{1,0:T(8,128)(2,1)} %param.38) | copy-start | bytes 6291460
  68.2 1.5 %copy-start.1 = (bf16[8,128,384]{2,1,0:T(8,128)(2,1)S(1)}, bf16[8,128,384]{2,1,0:T(8,128)(2,1)}, u32[]{:S(2)}) copy-start(bf16[8,128,384]{2,1,0:T(8,128)(2,1)} %shard_map.192) | copy-start | bytes 2359300

commit v6 on v5

--- a/solution.py
+++ b/solution.py
@@ -644,7 +644,9 @@
         scale = lax.rsqrt(jnp.mean(diff * diff, axis=-1, keepdims=True) + norm_eps)
         out_ref[at, :DV_A] = (diff * scale * mg_ref[...]).astype(bf16)
 
-    up = up_ref[:, pl.ds(pl.multiple_of(head * HDK, HDK), HDK)]
+    ups = up_ref[...].astype(f32)
+    chosen_head = lax.broadcasted_iota(jnp.int32, ups.shape, 1) == head
+    up = jnp.sum(jnp.where(chosen_head, ups, 0.0), axis=1).astype(bf16)
     bias = bias_ref[pl.ds(head, 1), :]
     r64 = lax.broadcasted_iota(jnp.int32, (BLK, BLK), 0)
     c64 = lax.broadcasted_iota(jnp.int32, (BLK, BLK), 1)
@@ -841,7 +843,7 @@
         projected,
         low_rank,
         retained,
-        decay_up.reshape(decay_up.shape[0], -1),
+        decay_up,
         decay_bias,
         query_gain[None],
         key_gain,

time: 73.7 us -> 72.2 us (0.980)
  local copies, waits for them, and re-layouts: 3.07 us -> 1.6 us
    unnamed x5 -> x4, local copies, waits for them, and re-layouts: 3.07 us -> 1.6 us
where the time goes in v6:
time: 72.2 us; the launch traced here: 71.9 us
  Pallas kernels  65.1 us (90%)
  matrix products  5.16 us (7%)
  local copies, waits for them, and re-layouts  1.6 us (2%)
    pallas_call x1, Pallas kernels, gather_positions(): pl.pallas_call(functools.partial(gather_kernel, n, fs_size, tp_size, hpd)...  33 us
    pallas_call x1, Pallas kernels, exchange_heads(): pl.pallas_call(functools.partial(exchange_kernel, n, fs_size, tp_size, hp...  24.5 us
    pallas_call x1, Pallas kernels, pair_body(): pl.pallas_call(functools.partial(mix_kernel, hpd, tp_size), out_shape=jax...  7.55 us
    dot_general x1, matrix products, pair_body(): jnp.einsum('htw,hwo->to', arrived[:, :, DV_A:], output_linear.reshape(hea...  3.69 us
    unnamed x4, local copies, waits for them, and re-layouts  1.6 us
    dot_general x1, matrix products, pair_body(): jnp.einsum('htw,hwo->to', arrived[:, :, :DV_A], output_attend.reshape(hea...  1.46 us

profile of v6, /device:TPU:11, one launch (start us, length us, event | category | flops | bytes accessed | tf_op | source)
XLA Modules:
  0.0 71.9 jit_solution(8354378838529603581)
XLA Ops:
  0.0 0.0 copy-start
  0.0 1.6 %copy-done = bf16[1024,1024]{1,0:T(8,128)(2,1)S(1)} copy-done((bf16[1024,1024]{1,0:T(8,128)(2,1)S(1)}, bf16[1024,1024]{1,0:T(8,128)(2,1)}, u32[]{:S(2)}) %copy-start) | copy-done | bytes 2097176
  1.6 33.0 %shard_map.190 = (bf16[512,896]{1,0:T(8,128)(2,1)}, bf16[512,32]{1,0:T(8,128)(2,1)}, f32[4,8,128]{2,1,0:T(8,128)}) custom-call(bf16[128,2048]{1,0:T(8,128)(2,1)} %bitcast.43, f32[8,128]{1,0:T(8,128)} %bitcast.46, f32[1,2048]{1,0:T(1,128)} %bitcast.45, bf16[32,2048]{1,0:T(8,128)(2,1)} %bitcast.44, bf16[4096,128]{1,0:T(8,128)(2,1)} %bitcast.38, ...), custom_call_target="tpu_custom_call" | custom-call | tf_op jit(solution)/shard_map/pallas_call | solution.py:531
  34.6 7.6 %shard_map.191.mix_ref = bf16[512,384]{1,0:T(8,128)(2,1)} custom-call(f32[8]{0:T(128)} %lam_ref.1, bf16[512,896]{1,0:T(8,128)(2,1)} %get-tuple-element.8.proj_ref, bf16[512,32]{1,0:T(8,128)(2,1)} %get-tuple-element.9.low_ref, f32[4,8,128]{2,1,0:T(8,128)} %get-tuple-element.10.ret_ref, bf16[32,8,128]{2,1,0:T(8,128)(2,1)} %up_ref.1, f32[8,128]{1,0:T(8,128)} %bias_ref.1, ...), custom_call_target="tpu_custom_call" | custom-call | tf_op jit(solution)/shard_map/pallas_call | solution.py:836
  42.2 24.5 %shard_map.192 = bf16[8,128,384]{2,1,0:T(8,128)(2,1)} custom-call(bf16[512,384]{1,0:T(8,128)(2,1)} %shard_map.191.mix_ref), custom_call_target="tpu_custom_call" | custom-call | tf_op jit(solution)/shard_map/pallas_call | solution.py:780
  66.7 0.0 copy-start.1
  66.7 1.5 %convolution_bitcast_fusion = f32[128,1024]{1,0:T(8,128)S(1)} fusion(bf16[8,128,1024]{2,1,0:T(8,128)(2,1)S(1)} %bitcast.35, bf16[8,128,384]{2,1,0:T(8,128)(2,1)} %shard_map.192), kind=kOutput, calls=%fused_computation | convolution fusion | flops 268435456 | bytes 2883584 | tf_op jit(solution)/shard_map/htw,hwo->to/dot_general | solution.py:856
  68.2 0.0 copy-done.1
  68.2 3.7 %fusion.2 = bf16[1,128,1024]{2,1,0:T(8,128)(2,1)} fusion(f32[128,1024]{1,0:T(8,128)S(1)} %convolution_bitcast_fusion, bf16[8,256,1024]{2,1,0:T(8,128)(2,1)} %bitcast.36, bf16[8,128,384]{2,1,0:T(8,128)(2,1)S(1)} %copy-done.1), kind=kOutput, calls=%fused_computation.4 | convolution fusion | flops 537133056 | bytes 5505024 | tf_op jit(solution)/shard_map/htw,hwo->to/dot_general | solution.py:861
Async XLA Ops:
  0.0 1.6 %copy-start = (bf16[1024,1024]{1,0:T(8,128)(2,1)S(1)}, bf16[1024,1024]{1,0:T(8,128)(2,1)}, u32[]{:S(2)}) copy-start(bf16[1024,1024]{1,0:T(8,128)(2,1)} %param.38) | copy-start | bytes 6291460
  66.7 1.5 %copy-start.1 = (bf16[8,128,384]{2,1,0:T(8,128)(2,1)S(1)}, bf16[8,128,384]{2,1,0:T(8,128)(2,1)}, u32[]{:S(2)}) copy-start(bf16[8,128,384]{2,1,0:T(8,128)(2,1)} %shard_map.192) | copy-start | bytes 2359300
